TPU v7x, 512 devices: a whole 4x4x16 slice. The times are simulated.
512 devices in a mesh: fs: 16 (over y, x), tp: 32 (over z, core).
Axes of the slice: x: 4, y: 4, z: 16, core: 2. Of those that a mesh axis runs over, the one named last changes fastest.
Arguments:
- saved_query_latent: bfloat16 [16384, 1536], P('fs', 'tp'), may hold values from -6 to 6
- saved_key_value_latent: bfloat16 [16384, 1024], P('fs', 'tp'), may hold values from -6 to 6
- query_cot: bfloat16 [16384, 6144], P('fs', 'tp'), may hold values from -0.046875 to 0.046875
- kv_cot: bfloat16 [16384, 8192], P('fs', 'tp'), may hold values from -0.046875 to 0.046875
- query_full_weight: float32 [1536, 6144], P('fs', 'tp'), may hold values from -0.6 to 0.6
- key_value_full_weight: float32 [1024, 8192], P('fs', 'tp'), may hold values from -0.6 to 0.6
- query_mom: float32 [1536, 6144], P('fs', 'tp'), may hold values from -50 to 50
- kv_mom: float32 [1024, 8192], P('fs', 'tp'), may hold values from -50 to 50
- query_left: bfloat16 [1536, 1536], P('fs'), may hold values from -1 to 1.5
- kv_left: bfloat16 [1024, 1024], P('fs'), may hold values from -1 to 1.5
- query_right: bfloat16 [32, 192, 192], P('tp'), may hold values from -1 to 1.5
- kv_right: bfloat16 [32, 256, 256], P('tp'), may hold values from -1 to 1.5
Outputs:
- query_mom_new: float32 [1536, 6144], P('fs', 'tp')
- kv_mom_new: float32 [1024, 8192], P('fs', 'tp')
- query_update: float32 [1536, 6144], P('fs', 'tp')
- kv_update: float32 [1024, 8192], P('fs', 'tp')
- query_weight: float32 [1536, 6144], P('fs', 'tp')
- kv_weight: float32 [1024, 8192], P('fs', 'tp')
- query_copy: bfloat16 [1536, 6144], P(None, 'tp')
- kv_copy: bfloat16 [1024, 8192], P(None, 'tp')
All inputs are finite; a program needn't handle non-finite values.
Results may differ from a plain program's by a relative error of at most 0.0055.
Values may be sent and summed in bfloat16 or wider, within the bound.
A program may use at most 64 MiB of HBM per device.

v0:
```python
import jax
import jax.numpy as jnp
from jax import lax
from jax.sharding import Mesh
from jax.sharding import PartitionSpec as P

FS = ("fs_0", "fs_1")
TP = ("tp_0", "tp_1")
FS_TP = ("fs_0", "fs_1", "tp_0", "tp_1")


beta_mom = 0.9
learn_rate = 0.01


def sent_to_all(shard, axis):
    copies = jnp.broadcast_to(shard, (lax.axis_size(axis), *shard.shape))
    return lax.all_to_all(copies, axis, split_axis=0, concat_axis=0, tiled=True)


def laid_out(parts, dim):
    dims = list(parts.shape[1:])
    dims[dim] *= parts.shape[0]
    return jnp.moveaxis(parts, 0, dim).reshape(dims)


def collect(shard, axis, dim):
    parts = sent_to_all(shard, axis)
    return laid_out(parts, dim)


def gathered_by_axis(shard, axes, dim):
    for axis in reversed(axes):
        shard = lax.all_gather(shard, axis, axis=dim, tiled=True)
    return shard


def gather_together(arrays, axis, dims):
    flat = jnp.concatenate([a.reshape(-1) for a in arrays])
    lines, at, finished = (lax.all_gather(flat, axis), 0, [])
    for a, dim in zip(arrays, dims):
        parts = lines[:, at : at + a.size].reshape(-1, *a.shape)
        finished.append(laid_out(parts, dim))
        at += a.size
    return tuple(finished)


def cut_along(shard, dim, size):
    before, after = (shard.shape[:dim], shard.shape[dim + 1 :])
    return jnp.moveaxis(shard.reshape(*before, size, -1, *after), dim, 0)


def sum_at_owner(shard, axis, dim):
    parts = cut_along(shard, dim, lax.axis_size(axis))
    arrived = lax.all_to_all(parts, axis, split_axis=0, concat_axis=0, tiled=True)
    return arrived.astype(jnp.float32).sum(axis=0)


def over_axes_2(shard, axes):
    for axis in axes:
        shard = lax.psum(shard, axis)
    return shard


def contract(latent, cotangent):
    return lax.dot_general(
        latent, cotangent, (((0,), (0,)), ((), ())), preferred_element_type=jnp.float32
    )


def left_product(half, left_rows, site_query):

    def accumulate(piece):
        return jnp.dot(left_rows, piece, preferred_element_type=jnp.float32)

    if site_query:
        return accumulate(collect(half, FS, 0))
    return accumulate(gathered_by_axis(half, FS, 0))


def right_product(left_half, right, width):
    rows = left_half.shape[0]
    heads_here = right.shape[0]
    blocks = left_half.reshape(rows, heads_here, width)
    pre = jnp.einsum("rhd,hde->rhe", blocks, right, preferred_element_type=jnp.float32)
    return pre.reshape(rows, heads_here * width)


def on_device(
    saved_query_latent,
    saved_key_value_latent,
    query_cot,
    kv_cot,
    query_full_weight,
    key_value_full_weight,
    query_mom,
    kv_mom,
    query_left,
    kv_left,
    query_right,
    kv_right,
):
    whole_query, whole_latent = gather_together(
        (saved_query_latent, saved_key_value_latent), TP, (1, 1)
    )
    query_grad = sum_at_owner(contract(whole_query, query_cot).astype(jnp.bfloat16), FS, 0)
    kv_grad = sum_at_owner(contract(whole_latent, kv_cot).astype(jnp.bfloat16), FS, 0)
    query_mom_new = beta_mom * query_mom + query_grad
    kv_mom_new = beta_mom * kv_mom + kv_grad
    query_msq = jnp.sum(query_mom_new * query_mom_new)
    kv_msq = jnp.sum(kv_mom_new * kv_mom_new)
    query_pre_left = left_product(query_mom_new.astype(jnp.bfloat16), query_left, True)
    kv_pre_left = left_product(kv_mom_new.astype(jnp.bfloat16), kv_left, False)
    query_pre = right_product(
        query_pre_left.astype(jnp.bfloat16), query_right, query_right.shape[1]
    )
    kv_pre = right_product(kv_pre_left.astype(jnp.bfloat16), kv_right, kv_right.shape[1])
    query_psq = jnp.sum(query_pre * query_pre)
    kv_psq = jnp.sum(kv_pre * kv_pre)
    query_msq, kv_msq, query_psq, kv_psq = (
        over_axes_2(query_msq, FS_TP),
        over_axes_2(kv_msq, FS_TP),
        over_axes_2(query_psq, FS_TP),
        over_axes_2(kv_psq, FS_TP),
    )
    query_update = jnp.sqrt(query_msq / query_psq) * query_pre
    kv_update = jnp.sqrt(kv_msq / kv_psq) * kv_pre
    query_weight = query_full_weight - learn_rate * query_update
    kv_weight = key_value_full_weight - learn_rate * kv_update
    query_copy, kv_copy = gather_together(
        (query_weight.astype(jnp.bfloat16), kv_weight.astype(jnp.bfloat16)), FS, (0, 0)
    )
    return (
        query_mom_new,
        kv_mom_new,
        query_update,
        kv_update,
        query_weight,
        kv_weight,
        query_copy,
        kv_copy,
    )


def solution(mesh):
    torus = Mesh(mesh.devices.reshape(4, 4, 16, 2), ("fs_0", "fs_1", "tp_0", "tp_1"))
    placed = (
        P(FS, TP),
        P(FS, TP),
        P(FS, TP),
        P(FS, TP),
        P(FS, TP),
        P(FS, TP),
        P(FS, TP),
        P(FS, TP),
        P(FS, None),
        P(FS, None),
        P(TP, None, None),
        P(TP, None, None),
    )
    return jax.shard_map(
        on_device,
        mesh=torus,
        in_specs=placed,
        out_specs=(
            P(FS, TP),
            P(FS, TP),
            P(FS, TP),
            P(FS, TP),
            P(FS, TP),
            P(FS, TP),
            P(None, TP),
            P(None, TP),
        ),
        check_vma=False,
    )
```

profile of v0, /device:TPU:1, one launch (start us, length us, event | category | flops | bytes accessed | tf_op | source)
XLA Modules:
  0.0 321.7 jit_solution(17623408891770891944)
XLA Ops:
  7.2 0.0 all-gather.5.cloned.1.call-start
  7.2 1.1 copy.26
  8.3 0.3 reshape.65
  8.7 1.0 copy.27
  9.7 0.2 reshape.66
  9.9 0.7 pad_maximum_fusion
  10.5 0.0 all-gather.5.cloned.1.call-update
  10.6 80.8 %all-gather.5.cloned.1.call-done = bf16[2621440]{0:T(1024)(128)(2,1)} async-done(((bf16[81920]{0:T(1024)(128)(2,1)}), bf16[2621440]{0:T(1024)(128)(2,1)}) %all-gather.5.cloned.1.call-update) | async-done | bytes 5242896 | tf_op jit(solution)/shard_map/all_gather | solution.py:40
  91.4 6.3 %reshape.78 = bf16[32,81920]{1,0:T(8,128)(2,1)} reshape(bf16[2621440]{0:T(1024)(128)(2,1)} %all-gather.5.cloned.1.call-done) | data formatting | bytes 10485760 | tf_op jit(solution)/shard_map/all_gather | solution.py:40
  97.7 1.6 slice-done
  99.3 8.0 %reshape.70 = bf16[32,1024,32]{2,1,0:T(8,128)(2,1)} reshape(bf16[32,32768]{1,0:T(8,128)(2,1)S(1)} %slice-done) | data formatting | bytes 4194304 | tf_op jit(solution)/shard_map/reshape | solution.py:42
  107.3 6.7 %copy.31 = bf16[1024,32,32]{0,2,1:T(8,128)(2,1)S(1)} copy(bf16[1024,32,32]{2,0,1:T(8,128)(2,1)} %bitcast.29) | data formatting | bytes 4194304 | tf_op jit(solution)/shard_map/transpose | solution.py:24
  114.0 1.5 convolution_convert_fusion.1
  115.5 6.5 %all-to-all-start.1 = ((bf16[16,64,256]{2,1,0:T(8,128)(2,1)}), bf16[16,64,256]{2,1,0:T(8,128)(2,1)S(1)}, u32[]{:S(2)}, u32[]{:S(2)}) async-start(bf16[16,64,256]{2,1,0:T(8,128)(2,1)} %bitcast.4), calls=%async_computation.1 | async-start | bytes 1048576 | tf_op jit(solution)/shard_map/all_to_all | solution.py:55
  122.1 3.8 %slice.16 = bf16[32,49152]{1,0:T(8,128)(2,1)} slice(bf16[32,81920]{1,0:T(8,128)(2,1)} %reshape.78), slice={[0:32], [0:49152]} | slice | bytes 6291456 | tf_op jit(solution)/shard_map/slice | solution.py:42
  125.9 10.9 %reshape.67 = bf16[32,1024,48]{2,1,0:T(8,128)(2,1)} reshape(bf16[32,49152]{1,0:T(8,128)(2,1)} %slice.16) | data formatting | bytes 6291456 | tf_op jit(solution)/shard_map/reshape | solution.py:42
  136.8 8.4 %copy.28 = bf16[1024,32,48]{0,2,1:T(8,128)(2,1)} copy(bf16[1024,32,48]{2,0,1:T(8,128)(2,1)} %bitcast.30) | data formatting | bytes 6291456 | tf_op jit(solution)/shard_map/transpose | solution.py:24
  145.1 3.1 convolution_convert_fusion
  148.2 0.7 reshape.69
  148.9 1.1 copy.29
  150.0 6.7 %all-to-all-start = ((bf16[16,96,192]{1,2,0:T(8,128)(2,1)}), bf16[16,96,192]{1,2,0:T(8,128)(2,1)S(1)}, u32[]{:S(2)}, u32[]{:S(2)}) async-start(bf16[16,96,192]{1,2,0:T(8,128)(2,1)} %copy.29), calls=%async_computation | async-start | bytes 1572864 | tf_op jit(solution)/shard_map/all_to_all | solution.py:55
  156.7 0.1 copy.25
  156.8 0.1 convert_reduce_fusion.1
  156.9 16.3 %all_gather.20 = bf16[256,256]{1,0:T(8,128)(2,1)S(1)} all-gather(bf16[64,256]{1,0:T(8,128)(2,1)S(1)} %get-tuple-element.46), channel_id=1, replica_groups=mesh['fs_0'=4,'fs_1'=4,'tp_0'=16,'tp_1'=2] {'fs_1'}, dimensions={0}, use_global_device_ids=true | all-gather | bytes 163840 | tf_op jit(solution)/shard_map/all_gather | solution.py:34
  173.2 0.2 convert_reduce_fusion
  173.4 0.6 multiply_reduce_fusion.1
  174.0 0.1 copy.32
  174.1 1.0 broadcast_in_dim.3
  175.1 5.0 %all-to-all-start.2 = ((bf16[16,96,192]{2,1,0:T(8,128)(2,1)}), bf16[16,96,192]{2,1,0:T(8,128)(2,1)S(1)}, u32[]{:S(2)}, u32[]{:S(2)}) async-start(bf16[16,96,192]{2,1,0:T(8,128)(2,1)} %broadcast_in_dim.3), calls=%async_computation.2 | async-start | bytes 1572864 | tf_op jit(solution)/shard_map/all_to_all | solution.py:18
  180.1 0.0 all-gather.7.cloned.1.call-start
  180.1 0.6 multiply_reduce_fusion.3
  180.8 17.6 %all_gather.21 = bf16[1024,256]{1,0:T(8,128)(2,1)S(1)} all-gather(bf16[256,256]{1,0:T(8,128)(2,1)S(1)} %all_gather.20), channel_id=1, replica_groups=mesh['fs_0'=4,'fs_1'=4,'tp_0'=16,'tp_1'=2] {'fs_0'}, dimensions={0}, use_global_device_ids=true | all-gather | bytes 655360 | tf_op jit(solution)/shard_map/all_gather | solution.py:34
  198.4 1.0 multiply_reduce_fusion.2
  199.3 1.2 multiply_reduce_fusion
  200.5 9.1 %all-reduce.2 = (f32[]{:T(128)}, f32[]{:T(128)}, f32[]{:T(128)}, f32[]{:T(128)}) all-reduce(f32[]{:T(128)} %get-tuple-element.48, f32[]{:T(128)} %get-tuple-element.50, f32[]{:T(128)} %multiply_reduce_fusion.3, f32[]{:T(128)} %get-tuple-element.52), channel_id=1, replica_groups=mesh['fs_0'=4,'fs_1'=4,'tp_0'=16,'tp_1'=2] {'fs_0'}, use_global_device_ids=true, to_apply=%region_3.0 | all-reduce | flops 4 | bytes 32 | tf_op jit(solution)/shard_map/psum | solution.py:61
  209.6 8.0 %all-reduce.1 = (f32[]{:T(128)}, f32[]{:T(128)}, f32[]{:T(128)}, f32[]{:T(128)}) all-reduce(f32[]{:T(128)} %get-tuple-element.32, f32[]{:T(128)} %get-tuple-element.33, f32[]{:T(128)} %get-tuple-element.34, f32[]{:T(128)} %get-tuple-element.35), channel_id=1, replica_groups=mesh['fs_0'=4,'fs_1'=4,'tp_0'=16,'tp_1'=2] {'fs_1'}, use_global_device_ids=true, to_apply=%region_4.0 | all-reduce | flops 4 | bytes 32 | tf_op jit(solution)/shard_map/psum | solution.py:61
  217.6 23.5 %all-reduce = (f32[]{:T(128)}, f32[]{:T(128)}, f32[]{:T(128)}, f32[]{:T(128)}) all-reduce(f32[]{:T(128)} %get-tuple-element.28, f32[]{:T(128)} %get-tuple-element.29, f32[]{:T(128)} %get-tuple-element.30, f32[]{:T(128)} %get-tuple-element.31), channel_id=1, replica_groups=mesh['fs_0'=4,'fs_1'=4,'tp_0'=16,'tp_1'=2] {'tp_0'}, use_global_device_ids=true, to_apply=%region_5.0 | all-reduce | flops 4 | bytes 32 | tf_op jit(solution)/shard_map/psum | solution.py:61
  241.1 16.8 %all-reduce.3 = (f32[]{:T(128)}, f32[]{:T(128)}, f32[]{:T(128)}, f32[]{:T(128)}) all-reduce(f32[]{:T(128)} %get-tuple-element.24, f32[]{:T(128)} %get-tuple-element.25, f32[]{:T(128)} %get-tuple-element.26, f32[]{:T(128)} %get-tuple-element.27), channel_id=1, replica_groups=mesh['fs_0'=4,'fs_1'=4,'tp_0'=16,'tp_1'=2] {'tp_1'}, use_global_device_ids=true, to_apply=%region_6.0 | all-reduce | flops 4 | bytes 32 | tf_op jit(solution)/shard_map/psum | solution.py:61
  260.7 0.7 convert_bitcast_fusion
  261.4 0.7 fusion.4
  262.1 0.1 reshape.76
  262.2 0.6 pad_maximum_fusion.1
  262.9 0.7 copy.33
  263.6 46.5 %all-gather.7.cloned.1.call-done = bf16[557056]{0:T(1024)(128)(2,1)} async-done(((bf16[34816]{0:T(1024)(128)(2,1)}), bf16[557056]{0:T(1024)(128)(2,1)}) %all-gather.7.cloned.1.call-update) | async-done | bytes 1114128 | tf_op jit(solution)/shard_map/all_gather | solution.py:40
  310.2 1.6 reshape.79
  311.8 1.0 reshape_reshape.7
  312.9 0.9 reshape_reshape.6
  313.8 1.1 copy.34
  (32 shorter events, 0.2 us)
Async XLA Ops:
  7.2 106.8 %copy-start = (bf16[1024,256]{1,0:T(8,128)(2,1)S(1)}, bf16[1024,256]{1,0:T(8,128)(2,1)}, u32[]{:S(2)}) copy-start(bf16[1024,256]{1,0:T(8,128)(2,1)} %param.15) | copy-start | bytes 1572868
  7.2 84.2 %all-gather.5.cloned.1.call-start = ((), (), s32[]{:S(2)}) async-start(), calls=%async_computation.3 | async-start | bytes 5406720 | tf_op jit(solution)/shard_map/all_gather | solution.py:40
  97.7 1.6 slice-start
  115.5 34.5 %all-to-all-start.1 = ((bf16[16,64,256]{2,1,0:T(8,128)(2,1)}), bf16[16,64,256]{2,1,0:T(8,128)(2,1)S(1)}, u32[]{:S(2)}, u32[]{:S(2)}) async-start(bf16[16,64,256]{2,1,0:T(8,128)(2,1)} %bitcast.4), calls=%async_computation.1 | async-start | bytes 1048576 | tf_op jit(solution)/shard_map/all_to_all | solution.py:55
  136.8 8.4 %copy-start.10 = (bf16[1024,192]{0,1:T(8,128)(2,1)S(1)}, bf16[1024,192]{0,1:T(8,128)(2,1)}, u32[]{:S(2)}) copy-start(bf16[1024,192]{0,1:T(8,128)(2,1)} %param.14) | copy-start | bytes 1179652
  148.2 8.5 %copy-start.6 = (f32[96,192]{1,0:T(8,128)S(1)}, f32[96,192]{1,0:T(8,128)}, u32[]{:S(2)}) copy-start(f32[96,192]{1,0:T(8,128)} %param.18) | copy-start | bytes 221188
  148.2 8.7 %copy-start.8 = (f32[64,256]{1,0:T(8,128)S(1)}, f32[64,256]{1,0:T(8,128)}, u32[]{:S(2)}) copy-start(f32[64,256]{1,0:T(8,128)} %param.19) | copy-start | bytes 196612
  150.0 23.2 %all-to-all-start = ((bf16[16,96,192]{1,2,0:T(8,128)(2,1)}), bf16[16,96,192]{1,2,0:T(8,128)(2,1)S(1)}, u32[]{:S(2)}, u32[]{:S(2)}) async-start(bf16[16,96,192]{1,2,0:T(8,128)(2,1)} %copy.29), calls=%async_computation | async-start | bytes 1572864 | tf_op jit(solution)/shard_map/all_to_all | solution.py:55
  156.7 41.7 %copy-start.3 = (bf16[1,256,256]{2,1,0:T(8,128)(2,1)S(1)}, bf16[1,256,256]{2,1,0:T(8,128)(2,1)}, u32[]{:S(2)}) copy-start(bf16[1,256,256]{2,1,0:T(8,128)(2,1)} %param.23) | copy-start | bytes 393220
  156.7 41.7 %copy-start.4 = (bf16[64,1024]{1,0:T(8,128)(2,1)S(1)}, bf16[64,1024]{1,0:T(8,128)(2,1)}, u32[]{:S(2)}) copy-start(bf16[64,1024]{1,0:T(8,128)(2,1)} %param.21) | copy-start | bytes 393220
  156.8 42.5 %copy-start.1 = (bf16[96,1536]{1,0:T(8,128)(2,1)S(1)}, bf16[96,1536]{1,0:T(8,128)(2,1)}, u32[]{:S(2)}) copy-start(bf16[96,1536]{1,0:T(8,128)(2,1)} %param.20) | copy-start | bytes 884740
  156.8 42.5 %copy-start.5 = (bf16[1,192,192]{2,1,0:T(8,128)(2,1)S(1)}, bf16[1,192,192]{2,1,0:T(8,128)(2,1)}, u32[]{:S(2)}) copy-start(bf16[1,192,192]{2,1,0:T(8,128)(2,1)} %param.22) | copy-start | bytes 221188
  156.9 43.6 %copy-start.2 = (f32[64,256]{1,0:T(8,128)}, f32[64,256]{1,0:T(8,128)S(1)}, u32[]{:S(2)}) copy-start(f32[64,256]{1,0:T(8,128)S(1)} %get-tuple-element.47) | copy-start | bytes 196612
  173.4 87.3 %copy-start.9 = (f32[64,256]{1,0:T(8,128)S(1)}, f32[64,256]{1,0:T(8,128)}, u32[]{:S(2)}) copy-start(f32[64,256]{1,0:T(8,128)} %param.17) | copy-start | bytes 196612
  173.4 88.0 %copy-start.7 = (f32[96,192]{1,0:T(8,128)S(1)}, f32[96,192]{1,0:T(8,128)}, u32[]{:S(2)}) copy-start(f32[96,192]{1,0:T(8,128)} %param.16) | copy-start | bytes 221188
  175.1 24.2 %all-to-all-start.2 = ((bf16[16,96,192]{2,1,0:T(8,128)(2,1)}), bf16[16,96,192]{2,1,0:T(8,128)(2,1)S(1)}, u32[]{:S(2)}, u32[]{:S(2)}) async-start(bf16[16,96,192]{2,1,0:T(8,128)(2,1)} %broadcast_in_dim.3), calls=%async_computation.2 | async-start | bytes 1572864 | tf_op jit(solution)/shard_map/all_to_all | solution.py:18
  180.1 130.1 %all-gather.7.cloned.1.call-start = ((), (), s32[]{:S(2)}) async-start(), calls=%async_computation.4 | async-start | bytes 1183744 | tf_op jit(solution)/shard_map/all_gather | solution.py:40
Sparse Core Ops, SparseCore 0:
  10.7 80.6 all-gather.4
  263.0 47.1 all-gather.6
where the time goes:
time: 323 us; the launch traced here: 322 us
  waiting for transfers between devices  127 us (39%)
  blocking collectives  91.3 us (28%)
  local copies, waits for them, and re-layouts  56.8 us (18%)
  starting transfers between devices  18.2 us (6%)
  between operations  17.1 us (5%)
  matrix products  6.72 us (2%)
  other arithmetic  4.17 us (1%)
    all_gather x2, waiting for transfers between devices, gather_together(): lines, at, finished = (lax.all_gather(flat, axis), 0, [])  127 us
    psum x4, blocking collectives, over_axes_2(): shard = lax.psum(shard, axis)  57.4 us
    all_gather x2, blocking collectives, gathered_by_axis(): shard = lax.all_gather(shard, axis, axis=dim, tiled=True)  33.9 us
    reshape x2, local copies, waits for them, and re-layouts, gather_together(): parts = lines[:, at:at + a.size].reshape(-1, *a.shape)  18.9 us
    transpose x2, local copies, waits for them, and re-layouts, laid_out(): return jnp.moveaxis(parts, 0, dim).reshape(dims)  15.1 us
    all_to_all x2, starting transfers between devices, sum_at_owner(): lax.all_to_all(parts, axis, split_axis=0, concat_axis=0, tiled=True)  13.2 us
    all_gather x2, local copies, waits for them, and re-layouts, gather_together(): lines, at, finished = (lax.all_gather(flat, axis), 0, [])  7.86 us
  transfers between devices with their start and end apart: 5, of which 2 were waited for; matrix products, arithmetic and copies ran while one was open for 9% of the time, Pallas kernels for 0%

commit v1 on v0

v1 whole, which is shorter than its diff:
```python
import functools

import jax
import jax.numpy as jnp
from jax import lax
from jax.experimental import pallas as pl
from jax.experimental.pallas import tpu as pltpu
from jax.sharding import Mesh
from jax.sharding import PartitionSpec as P

FS = ("fs_0", "fs_1")
TP = ("tp_0", "tp_1")

beta_mom = 0.9
learn_rate = 0.01

QR, KR = 96, 64
QW, KW = 192, 256
QF, KF = 48, 32
CF = QF + KF
MSG = 272
PIECES = ((0, 32), (32, 48), (48, 80))
N_Q_PIECES = 2
OWNER_DELAY = 3
F32, BF16 = jnp.float32, jnp.bfloat16


def dot(a, b):
    return jnp.dot(a, b, preferred_element_type=F32)


def dot_t(a, b):
    return lax.dot_general(a, b, (((1,), (1,)), ((), ())), preferred_element_type=F32)


def repeat_tail():
    row = lax.broadcasted_iota(jnp.int32, (QW, 256), 0)
    col = lax.broadcasted_iota(jnp.int32, (QW, 256), 1)
    return jnp.where(row == jnp.where(col < QW, col, col - 64), 1.0, 0.0).astype(BF16)


def pack(store, q, k):
    lane = lax.broadcasted_iota(jnp.int32, (QR // 2, 128), 1)
    store(0, q[:, :128].astype(BF16))
    tail = jnp.where(lane < 64, q[: QR // 2, 128:], q[QR // 2 :, 128:])
    store(96, tail.astype(BF16))
    store(144, k[:, :128].astype(BF16))
    store(208, k[:, 128:].astype(BF16))


def gather_kernel(
    ny, nx, nz,
    latq, latk, cotq, h_cotk, h_wq, h_wk, h_momq, h_momk, h_leftq, h_leftk, h_rightq, h_rightk,
    o_momq, o_momk, o_preq, o_prek, o_pre, o_w, o_sums,
    lat, cote, cotk, wq, wk, momq, momk, leftq, leftk, rightq, rightk,
    out_g, g, half, wfull, pfull, hq, hk, s_a, s_b,
    ring_recv, pair_recv, sems, load_sems,
):
    nf = ny * nx
    top = nz // 2
    y, x = lax.axis_index("fs_0"), lax.axis_index("fs_1")
    z, c = lax.axis_index("tp_0"), lax.axis_index("tp_1")
    fs = y * nx + x
    tp = z * 2 + c
    (ring_s, pair_s, g_s, g_r, h_s, h_r, w_s, w_r, p_s, p_r, a_s, a_r, b_s, b_r) = [
        sems.at[i] for i in range(14)
    ]

    def plane(d):
        t = lax.rem(fs + d, nf)
        return {"fs_0": t // nx, "fs_1": lax.rem(t, nx)}

    up, down = lax.rem(z + 1, nz), lax.rem(z + nz - 1, nz)

    loads = [
        pltpu.make_async_copy(src, dst, load_sems.at[i])
        for i, (src, dst) in enumerate(
            (
                (latq, lat.at[0, c, :QF]),
                (latk, lat.at[0, c, QF:]),
                (h_wq, wq),
                (h_wk, wk),
                (cotq, cote.at[:QW]),
                (cotq.at[128:], cote.at[QW:]),
                (h_cotk, cotk),
                (h_momq, momq),
                (h_momk, momk),
                (h_leftq, leftq),
                (h_leftk, leftk),
                (h_rightq, rightq),
                (h_rightk, rightk),
            )
        )
    ]
    for load in loads:
        load.start()

    barrier = pltpu.get_barrier_semaphore()
    for d in ({"tp_0": up}, {"tp_0": down}, {"tp_1": 1 - c}):
        pl.semaphore_signal(barrier, inc=1, device_id=d)
    for d in range(1, nf):
        pl.semaphore_signal(barrier, inc=1, device_id=plane(d))

    select = repeat_tail()

    def into(buffer, index):
        def store(at, value):
            buffer[index, at : at + value.shape[0], :] = value

        return store

    for load in loads[:4]:
        load.wait()
    pack(into(wfull, fs), dot(wq[...].astype(BF16), select), wk[...])

    pl.semaphore_wait(barrier, 3 + nf - 1)

    def send(src, dst, s_sem, r_sem, to):
        pltpu.make_async_remote_copy(
            src, dst, s_sem, r_sem, device_id=to, device_id_type=pl.DeviceIdType.MESH
        ).start()

    def wait(ref, sem):
        pltpu.make_async_copy(ref, ref, sem).wait()

    def part(slot, piece):
        lo, hi = PIECES[piece]
        return lat.at[slot, c, lo:hi]

    def forward(slot, to_slot, piece, to_z):
        send(
            part(slot, piece), part(to_slot, piece), ring_s,
            ring_recv.at[to_slot, piece], {"tp_0": to_z},
        )

    def share(slot, piece):
        send(part(slot, piece), part(slot, piece), pair_s, pair_recv.at[slot], {"tp_1": 1 - c})

    for p in range(len(PIECES)):
        forward(0, 1, p, up)
        forward(0, 2, p, down)
    for p in range(len(PIECES)):
        share(0, p)

    for load in loads[4:]:
        load.wait()
    delta = lax.rem(fs - z + nz, nz)
    own_step = jnp.minimum(delta, nz - delta)

    def partial_gradient(slot):
        wait(lat.at[slot, 1 - c], pair_recv.at[slot])
        lq = jnp.concatenate([lat[slot, 0, :QF, :], lat[slot, 1, :QF, :]], axis=0)
        lk = jnp.concatenate([lat[slot, 0, QF:, :], lat[slot, 1, QF:, :]], axis=0)
        pack(into(out_g, slot), dot_t(lq, cote[...]), dot(lk, cotk[...]))
        dist = (slot + 1) // 2
        owner = lax.rem(z + jnp.where(lax.rem(slot, 2) == 1, nz - dist, dist), nz)

        @pl.when(owner != fs)
        def _():
            send(
                out_g.at[slot], g.at[fs], g_s, g_r,
                {"fs_0": owner // nx, "fs_1": lax.rem(owner, nx)},
            )

        @pl.when(owner == fs)
        def _():
            g[fs] = out_g[slot]

    def momentum():
        wait(g.at[: nf - 1], g_r)
        total = g[0].astype(F32)
        for i in range(1, nf):
            total += g[i].astype(F32)
        tail = total[96:144]
        tail = jnp.concatenate([tail, pltpu.roll(tail, 64, 1)], axis=0)
        o_momq[:, :128] = beta_mom * momq[:, :128] + total[:96]
        o_momq[:, 128:] = beta_mom * momq[:, 128:] + tail[:, :64]
        o_momk[:, :128] = beta_mom * momk[:, :128] + total[144:208]
        o_momk[:, 128:] = beta_mom * momk[:, 128:] + total[208:272]
        pack(into(half, fs), dot(o_momq[...].astype(BF16), select), o_momk[...])
        for d in range(1, nf):
            send(half.at[fs], half.at[fs], h_s, h_r, plane(d))

    def step(k, carry):
        for p in range(len(PIECES)):
            is_q = p < N_Q_PIECES
            a, b = 2 * k - 1, jnp.minimum(2 * k, nz - 1)
            last_a, last_b = (top, top - 1) if is_q else (top - 1, top)

            @pl.when(k <= last_a)
            def _():
                wait(part(a, p), ring_recv.at[a, p])

                @pl.when(k < last_a)
                def _():
                    forward(a, a + 2, p, up)

                share(a, p)

            @pl.when(k <= last_b)
            def _():
                wait(part(b, p), ring_recv.at[b, p])

                @pl.when(k < last_b)
                def _():
                    forward(b, jnp.minimum(b + 2, nz - 1), p, down)

                share(b, p)

        for d in (2 * k - 1, 2 * k):

            @pl.when(d < nf)
            def _():
                send(wfull.at[fs], wfull.at[fs], w_s, w_r, plane(d))

        @pl.when(k >= 2)
        def _():
            partial_gradient(2 * k - 3)

        @pl.when(k <= top)
        def _():
            partial_gradient(2 * k - 2)

        @pl.when(k == jnp.minimum(own_step + OWNER_DELAY, top + 1))
        def _():
            momentum()

        return carry

    lax.fori_loop(1, top + 2, step, 0)

    wait(half.at[: nf - 1], h_r)

    def spread(s, carry):
        tail = half[s, 96:144, :]
        rolled = pltpu.roll(tail.astype(F32), 64, 1).astype(BF16)
        hq[s, :, :128] = half[s, :96, :]
        hq[s, :48, 128:] = tail
        hq[s, 48:, 128:] = rolled
        hk[s, :, :128] = half[s, 144:208, :]
        hk[s, :, 128:] = half[s, 208:272, :]
        return carry

    lax.fori_loop(0, nf, spread, 0)
    left_q = dot(leftq[...], hq[...].reshape(nf * QR, 256))[:, :QW].astype(BF16)
    left_k = dot(leftk[...], hk[...].reshape(nf * KR, 256)).astype(BF16)
    right_q = dot(rightq[0], select).astype(BF16)
    pre_q = dot(left_q, right_q)
    pre_k = dot(left_k, rightk[0])
    pack(into(pfull, fs), pre_q, pre_k)
    o_preq[...] = pre_q[:, :QW]
    o_prek[...] = pre_k
    lane = lax.broadcasted_iota(jnp.int32, (1, 128), 1)
    sums = jnp.zeros((1, 128), F32)
    for i, v in enumerate((o_momq[...], o_momk[...], pre_q[:, :QW], pre_k)):
        sums = jnp.where(lane == i, jnp.sum(v * v), sums)
    s_a[fs] = sums
    for d in range(1, nf):
        send(s_a.at[fs], s_a.at[fs], a_s, a_r, plane(d))
    for d in range(1, nf):
        send(pfull.at[fs], pfull.at[fs], p_s, p_r, plane(d))
    wait(s_a.at[: nf - 1], a_r)
    total = s_a[0]
    for i in range(1, nf):
        total += s_a[i]
    s_b[tp] = total

    def column(d):
        t = lax.rem(tp + d, 2 * nz)
        return {"tp_0": t // 2, "tp_1": lax.rem(t, 2)}

    for d in range(1, 2 * nz):
        send(s_b.at[tp], s_b.at[tp], b_s, b_r, column(d))
    wait(wfull.at[: nf - 1], w_r)
    wait(pfull.at[: nf - 1], p_r)
    o_w[...] = wfull[...]
    o_pre[...] = pfull[...]
    wait(s_b.at[: 2 * nz - 1], b_r)
    total = s_b[0]
    for i in range(1, 2 * nz):
        total += s_b[i]
    o_sums[...] = total

    wait(lat.at[: nz - 1, 0], ring_s)
    wait(lat.at[:, 0], pair_s)
    wait(out_g.at[: nf - 1], g_s)
    wait(half.at[: nf - 1], h_s)
    wait(wfull.at[: nf - 1], w_s)
    wait(pfull.at[: nf - 1], p_s)
    wait(s_a.at[: nf - 1], a_s)
    wait(s_b.at[: 2 * nz - 1], b_s)


def finish_kernel(
    nf, sums, preq, prek, pre, w, wq, wk, momq, momk,
    o_momq, o_momk, o_updq, o_updk, o_wq, o_wk, o_cq, o_ck, cq,
):
    v = sums[...]
    lane = lax.broadcasted_iota(jnp.int32, (1, 128), 1)
    scales = jnp.sqrt(v / pltpu.roll(v, 126, 1))
    scale_q, scale_k = [
        jnp.sum(jnp.where(lane == i, scales, 0.0), axis=1, keepdims=True) for i in (0, 1)
    ]
    o_momq[...] = momq[...]
    o_momk[...] = momk[...]
    upd_q = scale_q * preq[...]
    upd_k = scale_k * prek[...]
    o_updq[...] = upd_q
    o_updk[...] = upd_k
    o_wq[...] = wq[...] - learn_rate * upd_q
    o_wk[...] = wk[...] - learn_rate * upd_k

    def body(s, carry):
        q = w[s, :144, :].astype(F32) - learn_rate * (scale_q * pre[s, :144, :].astype(F32))
        k = w[s, 144:, :].astype(F32) - learn_rate * (scale_k * pre[s, 144:, :].astype(F32))
        tail = q[96:]
        cq[s, :, :128] = q[:96].astype(BF16)
        cq[s, :48, 128:] = tail.astype(BF16)
        cq[s, 48:, 128:] = pltpu.roll(tail, 64, 1).astype(BF16)
        rows = pl.ds(pl.multiple_of(s * KR, KR), KR)
        o_ck[rows, :128] = k[:64].astype(BF16)
        o_ck[rows, 128:] = k[64:].astype(BF16)
        return carry

    lax.fori_loop(0, nf, body, 0)
    row = lax.broadcasted_iota(jnp.int32, (QW, 256), 0)
    col = lax.broadcasted_iota(jnp.int32, (QW, 256), 1)
    eye = jnp.where(row == col, 1.0, 0.0).astype(BF16)
    o_cq[...] = dot_t(eye, cq[...].reshape(nf * QR, 256)).astype(BF16)


def on_device(
    ny, nx, nz,
    saved_query_latent,
    saved_key_value_latent,
    query_cot,
    kv_cot,
    query_full_weight,
    key_value_full_weight,
    query_mom,
    kv_mom,
    query_left,
    kv_left,
    query_right,
    kv_right,
):
    nf = ny * nx
    tokens = query_cot.shape[0]
    vmem = pl.BlockSpec(memory_space=pltpu.VMEM)
    shape = jax.ShapeDtypeStruct
    own_q, own_k = shape((QR, QW), F32), shape((KR, KW), F32)
    packed = shape((nf, MSG, 128), BF16)
    mom_q, mom_k, pre_q, pre_k, pre, w, sums = pl.pallas_call(
        functools.partial(gather_kernel, ny, nx, nz),
        out_shape=(own_q, own_k, own_q, own_k, packed, packed, shape((1, 128), F32)),
        in_specs=[pl.BlockSpec(memory_space=pltpu.HBM)] * 12,
        out_specs=(vmem,) * 7,
        scratch_shapes=[
            pltpu.VMEM((nz, 2, CF, tokens), BF16),
            pltpu.VMEM((256, tokens), BF16),
            pltpu.VMEM((tokens, KW), BF16),
            pltpu.VMEM((QR, QW), F32),
            pltpu.VMEM((KR, KW), F32),
            pltpu.VMEM((QR, QW), F32),
            pltpu.VMEM((KR, KW), F32),
            pltpu.VMEM((QR, nf * QR), BF16),
            pltpu.VMEM((KR, nf * KR), BF16),
            pltpu.VMEM((1, QW, QW), BF16),
            pltpu.VMEM((1, KW, KW), BF16),
            pltpu.VMEM((nz, MSG, 128), BF16),
            pltpu.VMEM((nf, MSG, 128), BF16),
            pltpu.VMEM((nf, MSG, 128), BF16),
            pltpu.VMEM((nf, MSG, 128), BF16),
            pltpu.VMEM((nf, MSG, 128), BF16),
            pltpu.VMEM((nf, QR, 256), BF16),
            pltpu.VMEM((nf, KR, 256), BF16),
            pltpu.VMEM((nf, 1, 128), F32),
            pltpu.VMEM((2 * nz, 1, 128), F32),
            pltpu.SemaphoreType.DMA((nz, len(PIECES))),
            pltpu.SemaphoreType.DMA((nz,)),
            pltpu.SemaphoreType.DMA((14,)),
            pltpu.SemaphoreType.DMA((13,)),
        ],
        compiler_params=pltpu.CompilerParams(
            collective_id=0, has_side_effects=True
        ),
    )(
        saved_query_latent.T, saved_key_value_latent.T, query_cot.T, kv_cot,
        query_full_weight, key_value_full_weight, query_mom, kv_mom,
        query_left, kv_left, query_right, kv_right,
    )
    outs = pl.pallas_call(
        functools.partial(finish_kernel, nf),
        out_shape=(
            own_q, own_k, own_q, own_k, own_q, own_k,
            shape((QW, nf * QR), BF16), shape((nf * KR, KW), BF16),
        ),
        in_specs=[vmem] * 9,
        out_specs=(vmem,) * 8,
        scratch_shapes=[pltpu.VMEM((nf, QR, 256), BF16)],
        compiler_params=pltpu.CompilerParams(vmem_limit_bytes=32 * 2**20),
    )(sums, pre_q, pre_k, pre, w, query_full_weight, key_value_full_weight, mom_q, mom_k)
    return (*outs[:6], outs[6].T, outs[7])


def solution(mesh, dims=(4, 4, 16)):
    torus = Mesh(mesh.devices.reshape(*dims, 2), (*FS, *TP))
    placed = (P(FS, TP),) * 8 + (P(FS, None),) * 2 + (P(TP, None, None),) * 2
    return jax.shard_map(
        functools.partial(on_device, *dims),
        mesh=torus,
        in_specs=placed,
        out_specs=(P(FS, TP),) * 6 + (P(None, TP),) * 2,
        check_vma=False,
    )
```

time: 323 us -> 129 us (0.40)
  waiting for transfers between devices: 127 us -> 0 us
  Pallas kernels: 0 us -> 122 us
  blocking collectives: 91.3 us -> 0 us
  local copies, waits for them, and re-layouts: 56.8 us -> 6.63 us
  starting transfers between devices: 18.2 us -> 0 us
  between operations: 17.1 us -> 0.69 us
  matrix products: 6.72 us -> 0 us
  other arithmetic: 4.17 us -> 0 us
    all_gather x2 -> x0, waiting for transfers between devices: 127 us -> none  [gather_together(): lines, at, finished = (lax.all_gather(flat, axis), 0, [])]
    pallas_call x0 -> x2, Pallas kernels: none -> 122 us  [the longest x1 119 us: on_device(): pl.pallas_call(functools.partial(gather_kernel, ny, nx, nz), out_shape=(o...]
    psum x4 -> x0, blocking collectives: 57.4 us -> none  [over_axes_2(): shard = lax.psum(shard, axis)]
    all_gather x2 -> x0, blocking collectives: 33.9 us -> none  [gathered_by_axis(): shard = lax.all_gather(shard, axis, axis=dim, tiled=True)]
    reshape x7 -> x0, local copies, waits for them, and re-layouts: 21.3 us -> none  [the longest x2 18.9 us: gather_together(): parts = lines[:, at:at + a.size].reshape(-1, *a.shape)]
    all_to_all x3 -> x0, starting transfers between devices: 18.2 us -> none  [the longest x2 13.2 us: sum_at_owner(): lax.all_to_all(parts, axis, split_axis=0, concat_axis=0, tiled=True)]
    transpose x2 -> x0, local copies, waits for them, and re-layouts: 15.1 us -> none  [laid_out(): return jnp.moveaxis(parts, 0, dim).reshape(dims)]
    all_gather x2 -> x0, local copies, waits for them, and re-layouts: 7.86 us -> none  [gather_together(): lines, at, finished = (lax.all_gather(flat, axis), 0, [])]
  transfers between devices with their start and end apart: 5 -> 0, of which waited for: 2 -> 0; matrix products, arithmetic and copies ran while one was open for 9% -> 0% of each run, Pallas kernels for 0% -> 0%
where the time goes in v1:
time: 129 us
  Pallas kernels  122 us (95%)
  local copies, waits for them, and re-layouts  6.63 us (5%)
    pallas_call x1, Pallas kernels, on_device(): pl.pallas_call(functools.partial(gather_kernel, ny, nx, nz), out_shape=(o...  119 us
    unnamed x18, local copies, waits for them, and re-layouts  6.63 us
    pallas_call x1, Pallas kernels, on_device(): pl.pallas_call(functools.partial(finish_kernel, nf), out_shape=(own_q, ow...  3.05 us

profile of v1, /device:TPU:1, one launch (start us, length us, event | category | flops | bytes accessed | tf_op | source)
XLA Modules:
  0.0 129.0 jit_solution(1774910308613285127)
XLA Ops:
  0.6 0.0 copy-start.3
  0.6 0.0 copy-start.2
  0.7 118.7 %shard_map.179 = (f32[96,192]{1,0:T(8,128)}, f32[64,256]{1,0:T(8,128)}, f32[96,192]{1,0:T(8,128)}, f32[64,256]{1,0:T(8,128)}, bf16[16,272,128]{2,1,0:T(8,128)(2,...) custom-call(bf16[48,1024]{1,0:T(8,128)(2,1)} %bitcast.5, bf16[32,1024]{1,0:T(8,128)(2,1)} %bitcast.6, ...), custom_call_target="tpu_custom_call" | custom-call | tf_op jit(solution)/shard_map/pallas_call | solution.py:353
  119.3 0.0 copy-done.3
  119.4 0.0 copy-done.2
  119.4 0.0 copy-start
  119.4 1.2 copy-done
  120.6 0.0 copy-start.1
  120.6 1.2 copy-done.1
  121.9 0.0 copy-start.4
  121.9 0.9 copy-done.4
  122.8 0.0 copy-start.5
  122.8 0.9 copy-done.5
  123.6 0.0 copy-start.6
  123.7 0.8 copy-done.6
  124.5 0.0 copy-start.7
  124.5 0.8 copy-done.7
  125.3 0.0 copy-start.8
  125.3 0.7 copy-done.8
  126.0 3.0 %shard_map.180 = (f32[96,192]{1,0:T(8,128)}, f32[64,256]{1,0:T(8,128)}, f32[96,192]{1,0:T(8,128)}, f32[64,256]{1,0:T(8,128)}, f32[96,192]{1,0:T(8,128)}, /*index...) custom-call(f32[1,128]{1,0:T(1,128)S(1)} %copy-done.8, f32[96,192]{1,0:T(8,128)S(1)} %copy-done.5, ...), custom_call_target="tpu_custom_call" | custom-call | tf_op jit(solution)/shard_map/pallas_call | solution.py:392
Async XLA Ops:
  0.6 118.7 %copy-start.3 = (f32[64,256]{1,0:T(8,128)S(1)}, f32[64,256]{1,0:T(8,128)}, u32[]{:S(2)}) copy-start(f32[64,256]{1,0:T(8,128)} %wk.1) | copy-start | bytes 196612
  0.6 118.7 %copy-start.2 = (f32[96,192]{1,0:T(8,128)S(1)}, f32[96,192]{1,0:T(8,128)}, u32[]{:S(2)}) copy-start(f32[96,192]{1,0:T(8,128)} %wq.1) | copy-start | bytes 221188
  119.4 1.2 copy-start
  120.6 1.2 copy-start.1
  121.9 0.9 copy-start.4
  122.8 0.9 copy-start.5
  123.6 0.8 copy-start.6
  124.5 0.8 copy-start.7
  125.3 0.7 copy-start.8

commit v2 on v1

v2 whole, which is shorter than its diff:
```python
import functools

import jax
import jax.numpy as jnp
from jax import lax
from jax.experimental import pallas as pl
from jax.experimental.pallas import tpu as pltpu
from jax.sharding import Mesh
from jax.sharding import PartitionSpec as P

FS = ("fs_0", "fs_1")
TP = ("tp_0", "tp_1")

beta_mom = 0.9
learn_rate = 0.01

QR, KR = 96, 64
QW, KW = 192, 256
QF, KF = 48, 32
CF = QF + KF
QP, KP = 144, 128
PIECES = ((0, 32), (32, 48), (48, 80))
N_Q_PIECES = 2
DELAY = 2
F32, BF16 = jnp.float32, jnp.bfloat16


def dot(a, b):
    return jnp.dot(a, b, preferred_element_type=F32)


def dot_t(a, b):
    return lax.dot_general(a, b, (((1,), (1,)), ((), ())), preferred_element_type=F32)


def repeat_tail():
    row = lax.broadcasted_iota(jnp.int32, (QW, 256), 0)
    col = lax.broadcasted_iota(jnp.int32, (QW, 256), 1)
    return jnp.where(row == jnp.where(col < QW, col, col - 64), 1.0, 0.0).astype(BF16)


def pack_q(q):
    lane = lax.broadcasted_iota(jnp.int32, (QR // 2, 128), 1)
    tail = jnp.where(lane < 64, q[: QR // 2, 128:], q[QR // 2 :, 128:])
    return jnp.concatenate([q[:, :128], tail], axis=0).astype(BF16)


def pack_k(k):
    return jnp.concatenate([k[:, :128], k[:, 128:]], axis=0).astype(BF16)


def both(*conditions):
    return functools.reduce(jnp.logical_and, conditions)


def gather_kernel(
    ny, nx, nz,
    latq, latk, cotq, h_cotk, h_wq, h_wk, h_momq, h_momk, h_leftq, h_leftk, h_rightq, h_rightk,
    o_momq, o_momk, o_preq, o_prek, o_pq, o_pk, o_bq, o_bk, o_sums,
    lat, cote, cotk, wq, wk, momq, momk, leftq, leftk, rightq, rightk,
    outq, outk, rowq, rowk, midq, midk, ownq, ownk,
    halfq, halfk, wallq, wallk, pallq, pallk, hq, hk, s_a, s_b,
    ring_recv, pair_recv, row_recv, col_recv, cast_recv, sems, load_sems,
):
    nf = ny * nx
    top = nz // 2
    y, x = lax.axis_index("fs_0"), lax.axis_index("fs_1")
    z, c = lax.axis_index("tp_0"), lax.axis_index("tp_1")
    fs = y * nx + x
    tp = z * 2 + c
    ring_s, pair_s, g0q, g0k, g1q, g1k, r1q, r1k, a_s, a_r, b_s, b_r = [
        sems.at[i] for i in range(12)
    ]

    def row_peer(d):
        return {"fs_1": lax.rem(x + d, nx)}

    def col_peer(d):
        return {"fs_0": lax.rem(y + d, ny)}

    def plane(d):
        t = lax.rem(fs + d, nf)
        return {"fs_0": t // nx, "fs_1": lax.rem(t, nx)}

    up, down = lax.rem(z + 1, nz), lax.rem(z + nz - 1, nz)

    loads = [
        pltpu.make_async_copy(src, dst, load_sems.at[i])
        for i, (src, dst) in enumerate(
            (
                (latq, lat.at[0, c, :QF]),
                (latk, lat.at[0, c, QF:]),
                (h_wq, wq),
                (h_wk, wk),
                (cotq, cote.at[:QW]),
                (cotq.at[128:], cote.at[QW:]),
                (h_cotk, cotk),
                (h_momq, momq),
                (h_momk, momk),
                (h_leftq, leftq),
                (h_leftk, leftk),
                (h_rightq, rightq),
                (h_rightk, rightk),
            )
        )
    ]
    for load in loads:
        load.start()

    barrier = pltpu.get_barrier_semaphore()
    for d in ({"tp_0": up}, {"tp_0": down}, {"tp_1": 1 - c}):
        pl.semaphore_signal(barrier, inc=1, device_id=d)
    for d in range(1, nf):
        pl.semaphore_signal(barrier, inc=1, device_id=plane(d))

    select = repeat_tail()

    for load in loads[:4]:
        load.wait()
    wallq[fs] = pack_q(dot(wq[...].astype(BF16), select))
    wallk[fs] = pack_k(wk[...])

    pl.semaphore_wait(barrier, 3 + nf - 1)

    def send(src, dst, s_sem, r_sem, to):
        pltpu.make_async_remote_copy(
            src, dst, s_sem, r_sem, device_id=to, device_id_type=pl.DeviceIdType.MESH
        ).start()

    def wait(ref, sem):
        pltpu.make_async_copy(ref, ref, sem).wait()

    def part(slot, piece):
        lo, hi = PIECES[piece]
        return lat.at[slot, c, lo:hi]

    def forward(slot, to_slot, piece, to_z):
        send(
            part(slot, piece), part(to_slot, piece), ring_s,
            ring_recv.at[to_slot, piece], {"tp_0": to_z},
        )

    def share(slot, piece):
        send(part(slot, piece), part(slot, piece), pair_s, pair_recv.at[slot], {"tp_1": 1 - c})

    for p in range(len(PIECES)):
        forward(0, 1, p, up)
        forward(0, 2, p, down)
    for p in range(len(PIECES)):
        share(0, p)

    class Cast:
        def __init__(self, which, q, k):
            self.q, self.k = q, k
            self.which = which
            self.sq, self.sk, self.rq, self.rk = [cast_recv.at[which, i] for i in range(4)]

        def along_x(self, block, s_sem, r_sem):
            for d in range(1, nx):
                send(block, block, s_sem, r_sem, row_peer(d))

        def along_y(self, block, s_sem, r_sem):
            for d in range(1, ny):
                send(block, block, s_sem, r_sem, col_peer(d))

        def start(self):
            q, k = self.q.at[fs], self.k.at[fs]
            self.along_x(q, self.sq, row_recv.at[self.which, x])
            self.along_y(k, self.sk, col_recv.at[self.which, y])
            self.along_y(q, self.sq, self.rq)
            self.along_x(k, self.sk, self.rk)

        def pass_q(self, xs):
            block = self.q.at[y * nx + xs]
            wait(block, row_recv.at[self.which, xs])
            self.along_y(block, self.sq, self.rq)

        def pass_k(self, ys):
            block = self.k.at[ys * nx + x]
            wait(block, col_recv.at[self.which, ys])
            self.along_x(block, self.sk, self.rk)

        def finish(self):
            wait(self.q.at[: (ny - 1) * nx], self.rq)
            wait(self.k.at[: (nx - 1) * ny], self.rk)

        def drain(self):
            wait(self.q.at[: nf - 1], self.sq)
            wait(self.k.at[: nf - 1], self.sk)

    weights, halves, pres = Cast(0, wallq, wallk), Cast(1, halfq, halfk), Cast(2, pallq, pallk)
    weights.start()

    for load in loads[4:]:
        load.wait()
    delta = lax.rem(fs - z + nz, nz)
    own_step = jnp.minimum(delta, nz - delta)

    def partial_gradient(slot, s):
        wait(lat.at[slot, 1 - c], pair_recv.at[slot])
        lq = jnp.concatenate([lat[slot, 0, :QF, :], lat[slot, 1, :QF, :]], axis=0)
        lk = jnp.concatenate([lat[slot, 0, QF:, :], lat[slot, 1, QF:, :]], axis=0)
        outq[slot] = pack_q(dot_t(lq, cote[...]))
        outk[slot] = pack_k(dot(lk, cotk[...]))
        ys, xs = s // nx, lax.rem(s, nx)

        @pl.when(xs != x)
        def _():
            send(outq.at[slot], rowq.at[ys, x], g0q, pair_recv.at[nz + ys], {"fs_1": xs})

        @pl.when(xs == x)
        def _():
            rowq[ys, x] = outq[slot]

        @pl.when(ys != y)
        def _():
            send(outk.at[slot], rowk.at[xs, y], g0k, pair_recv.at[nz + ny + xs], {"fs_0": ys})

        @pl.when(ys == y)
        def _():
            rowk[xs, y] = outk[slot]

    def added(ref, index, n):
        total = ref[index, 0].astype(F32)
        for i in range(1, n):
            total += ref[index, i].astype(F32)
        return total

    def reduce_first(slot, s):
        ys, xs = s // nx, lax.rem(s, nx)

        @pl.when(xs == x)
        def _():
            wait(rowq.at[ys, : nx - 1], pair_recv.at[nz + ys])
            total = added(rowq, ys, nx).astype(BF16)

            @pl.when(ys != y)
            def _():
                midq[ys] = total
                send(midq.at[ys], ownq.at[0, y], g1q, r1q, {"fs_0": ys})

            @pl.when(ys == y)
            def _():
                ownq[0, y] = total

        @pl.when(ys == y)
        def _():
            wait(rowk.at[xs, : ny - 1], pair_recv.at[nz + ny + xs])
            total = added(rowk, xs, ny).astype(BF16)

            @pl.when(xs != x)
            def _():
                midk[xs] = total
                send(midk.at[xs], ownk.at[0, x], g1k, r1k, {"fs_1": xs})

            @pl.when(xs == x)
            def _():
                ownk[0, x] = total

    def momentum():
        wait(ownq.at[0, : ny - 1], r1q)
        wait(ownk.at[0, : nx - 1], r1k)
        q, k = added(ownq, 0, ny), added(ownk, 0, nx)
        tail = q[QR:]
        tail = jnp.concatenate([tail, pltpu.roll(tail, 64, 1)], axis=0)
        o_momq[:, :128] = beta_mom * momq[:, :128] + q[:QR]
        o_momq[:, 128:] = beta_mom * momq[:, 128:] + tail[:, :64]
        o_momk[:, :128] = beta_mom * momk[:, :128] + k[:KR]
        o_momk[:, 128:] = beta_mom * momk[:, 128:] + k[KR:]
        halfq[fs] = pack_q(dot(o_momq[...].astype(BF16), select))
        halfk[fs] = pack_k(o_momk[...])
        halves.start()

    def relay(slot, s):
        ys, xs = s // nx, lax.rem(s, nx)

        @pl.when(both(ys == y, xs != x))
        def _():
            halves.pass_q(xs)

        @pl.when(both(xs == x, ys != y))
        def _():
            halves.pass_k(ys)

    def per_slot(do, st):
        @pl.when(both(st >= 1, st <= top))
        def _():
            do(2 * st - 1, lax.rem(z + nz - st, nz))

        @pl.when(both(st >= 0, st < top))
        def _():
            do(2 * st, lax.rem(z + st, nz))

    def step(k, carry):
        for p in range(len(PIECES)):
            is_q = p < N_Q_PIECES
            a, b = 2 * k - 1, jnp.minimum(2 * k, nz - 1)
            last_a, last_b = (top, top - 1) if is_q else (top - 1, top)

            @pl.when(k <= last_a)
            def _():
                wait(part(a, p), ring_recv.at[a, p])

                @pl.when(k < last_a)
                def _():
                    forward(a, a + 2, p, up)

                share(a, p)

            @pl.when(k <= last_b)
            def _():
                wait(part(b, p), ring_recv.at[b, p])

                @pl.when(k < last_b)
                def _():
                    forward(b, jnp.minimum(b + 2, nz - 1), p, down)

                share(b, p)

        for i in range(1, max(nx, ny)):

            @pl.when(k == i + 2)
            def _():
                if i < nx:
                    weights.pass_q(lax.rem(x + i, nx))
                if i < ny:
                    weights.pass_k(lax.rem(y + i, ny))

        per_slot(partial_gradient, k - 1)
        per_slot(reduce_first, k - 1 - DELAY)

        @pl.when(k == own_step + 1 + 2 * DELAY)
        def _():
            momentum()

        per_slot(relay, k - 1 - 3 * DELAY)
        return carry

    lax.fori_loop(1, max(top + 2 + 3 * DELAY, max(nx, ny) + 2), step, 0)

    weights.finish()
    w_out = [
        pltpu.make_async_copy(wallq, o_bq, load_sems.at[0]),
        pltpu.make_async_copy(wallk, o_bk, load_sems.at[1]),
    ]
    for copy in w_out:
        copy.start()
    halves.finish()

    def spread(s, carry):
        tail = halfq[s, QR:, :]
        hq[s, :, :128] = halfq[s, :QR, :]
        hq[s, : QR // 2, 128:] = tail
        hq[s, QR // 2 :, 128:] = pltpu.roll(tail.astype(F32), 64, 1).astype(BF16)
        hk[s, :, :128] = halfk[s, :KR, :]
        hk[s, :, 128:] = halfk[s, KR:, :]
        return carry

    lax.fori_loop(0, nf, spread, 0)
    left_q = dot(leftq[...], hq[...].reshape(nf * QR, 256))[:, :QW].astype(BF16)
    left_k = dot(leftk[...], hk[...].reshape(nf * KR, 256)).astype(BF16)
    right_q = dot(rightq[0], select).astype(BF16)
    pre_q = dot(left_q, right_q)
    pre_k = dot(left_k, rightk[0])
    pallq[fs] = pack_q(pre_q)
    pallk[fs] = pack_k(pre_k)
    o_preq[...] = pre_q[:, :QW]
    o_prek[...] = pre_k
    lane = lax.broadcasted_iota(jnp.int32, (1, 128), 1)
    sums = jnp.zeros((1, 128), F32)
    for i, v in enumerate((o_momq[...], o_momk[...], pre_q[:, :QW], pre_k)):
        sums = jnp.where(lane == i, jnp.sum(v * v), sums)
    s_a[fs] = sums
    for d in range(1, nf):
        send(s_a.at[fs], s_a.at[fs], a_s, a_r, plane(d))
    pres.start()
    wait(s_a.at[: nf - 1], a_r)
    total = s_a[0]
    for i in range(1, nf):
        total += s_a[i]
    s_b[tp] = total

    def column(d):
        t = lax.rem(tp + d, 2 * nz)
        return {"tp_0": t // 2, "tp_1": lax.rem(t, 2)}

    for d in range(1, 2 * nz):
        send(s_b.at[tp], s_b.at[tp], b_s, b_r, column(d))
    for i in range(1, nx):
        pres.pass_q(lax.rem(x + i, nx))
    for i in range(1, ny):
        pres.pass_k(lax.rem(y + i, ny))
    pres.finish()
    p_out = [
        pltpu.make_async_copy(pallq, o_pq, load_sems.at[2]),
        pltpu.make_async_copy(pallk, o_pk, load_sems.at[3]),
    ]
    for copy in p_out:
        copy.start()
    wait(lat.at[: nz - 1, 0], ring_s)
    wait(lat.at[:, 0], pair_s)
    wait(outq.at[: nf - ny], g0q)
    wait(outk.at[: nf - nx], g0k)
    wait(midq.at[: ny - 1], g1q)
    wait(midk.at[: nx - 1], g1k)
    weights.drain()
    halves.drain()
    pres.drain()
    for copy in (*w_out, *p_out):
        copy.wait()
    wait(s_a.at[: nf - 1], a_s)
    wait(s_b.at[: 2 * nz - 1], b_s)
    wait(s_b.at[: 2 * nz - 1], b_r)
    total = s_b[0]
    for i in range(1, 2 * nz):
        total += s_b[i]
    o_sums[...] = total


def finish_kernel(
    nf, *refs,
):
    given, outs, held = refs[:11], refs[11:19], refs[19:30]
    cq, load_sems = refs[30:]
    o_momq, o_momk, o_updq, o_updk, o_wq, o_wk, o_cq, o_ck = outs
    loads = [
        pltpu.make_async_copy(src, dst, load_sems.at[i])
        for i, (src, dst) in enumerate(zip(given, held))
    ]
    for load in loads:
        load.start()
    row = lax.broadcasted_iota(jnp.int32, (QW, 256), 0)
    col = lax.broadcasted_iota(jnp.int32, (QW, 256), 1)
    eye = jnp.where(row == col, 1.0, 0.0).astype(BF16)
    for load in loads:
        load.wait()
    sums, preq, prek, pq, pk, bq, bk, wq, wk, momq, momk = held
    v = sums[...]
    lane = lax.broadcasted_iota(jnp.int32, (1, 128), 1)
    scales = jnp.sqrt(v / pltpu.roll(v, 126, 1))
    scale_q, scale_k = [
        jnp.sum(jnp.where(lane == i, scales, 0.0), axis=1, keepdims=True) for i in (0, 1)
    ]
    o_momq[...] = momq[...]
    o_momk[...] = momk[...]
    upd_q = scale_q * preq[...]
    upd_k = scale_k * prek[...]
    o_updq[...] = upd_q
    o_updk[...] = upd_k
    o_wq[...] = wq[...] - learn_rate * upd_q
    o_wk[...] = wk[...] - learn_rate * upd_k

    def body(s, carry):
        q = bq[s].astype(F32) - learn_rate * (scale_q * pq[s].astype(F32))
        k = bk[s].astype(F32) - learn_rate * (scale_k * pk[s].astype(F32))
        tail = q[QR:]
        cq[s, :, :128] = q[:QR].astype(BF16)
        cq[s, : QR // 2, 128:] = tail.astype(BF16)
        cq[s, QR // 2 :, 128:] = pltpu.roll(tail, 64, 1).astype(BF16)
        rows = pl.ds(pl.multiple_of(s * KR, KR), KR)
        o_ck[rows, :128] = k[:KR].astype(BF16)
        o_ck[rows, 128:] = k[KR:].astype(BF16)
        return carry

    lax.fori_loop(0, nf, body, 0)
    o_cq[...] = dot_t(eye, cq[...].reshape(nf * QR, 256)).astype(BF16)


def on_device(
    ny, nx, nz,
    saved_query_latent,
    saved_key_value_latent,
    query_cot,
    kv_cot,
    query_full_weight,
    key_value_full_weight,
    query_mom,
    kv_mom,
    query_left,
    kv_left,
    query_right,
    kv_right,
):
    nf = ny * nx
    tokens = query_cot.shape[0]
    vmem = pl.BlockSpec(memory_space=pltpu.VMEM)
    shape = jax.ShapeDtypeStruct
    own_q, own_k = shape((QR, QW), F32), shape((KR, KW), F32)
    all_q, all_k = shape((nf, QP, 128), BF16), shape((nf, KP, 128), BF16)
    row = shape((1, 128), F32)
    hbm = pl.BlockSpec(memory_space=pltpu.HBM)
    block_q, block_k = [lambda *n, r=r: pltpu.VMEM((*n, r, 128), BF16) for r in (QP, KP)]
    dma = pltpu.SemaphoreType.DMA
    mom_q, mom_k, pre_q, pre_k, p_q, p_k, b_q, b_k, sums = pl.pallas_call(
        functools.partial(gather_kernel, ny, nx, nz),
        out_shape=(own_q, own_k, own_q, own_k, all_q, all_k, all_q, all_k, row),
        in_specs=[hbm] * 12,
        out_specs=(vmem,) * 4 + (hbm,) * 4 + (vmem,),
        scratch_shapes=[
            pltpu.VMEM((nz, 2, CF, tokens), BF16),
            pltpu.VMEM((256, tokens), BF16),
            pltpu.VMEM((tokens, KW), BF16),
            pltpu.VMEM((QR, QW), F32),
            pltpu.VMEM((KR, KW), F32),
            pltpu.VMEM((QR, QW), F32),
            pltpu.VMEM((KR, KW), F32),
            pltpu.VMEM((QR, nf * QR), BF16),
            pltpu.VMEM((KR, nf * KR), BF16),
            pltpu.VMEM((1, QW, QW), BF16),
            pltpu.VMEM((1, KW, KW), BF16),
            block_q(nz),
            block_k(nz),
            block_q(ny, nx),
            block_k(nx, ny),
            block_q(ny),
            block_k(nx),
            block_q(1, ny),
            block_k(1, nx),
            *(block_q(nf), block_k(nf)) * 3,
            pltpu.VMEM((nf, QR, 256), BF16),
            pltpu.VMEM((nf, KR, 256), BF16),
            pltpu.VMEM((nf, 1, 128), F32),
            pltpu.VMEM((2 * nz, 1, 128), F32),
            dma((nz, len(PIECES))),
            dma((nz + ny + nx,)),
            dma((3, nx)),
            dma((3, ny)),
            dma((3, 4)),
            dma((12,)),
            dma((13,)),
        ],
        compiler_params=pltpu.CompilerParams(collective_id=0, has_side_effects=True),
    )(
        saved_query_latent.T, saved_key_value_latent.T, query_cot.T, kv_cot,
        query_full_weight, key_value_full_weight, query_mom, kv_mom,
        query_left, kv_left, query_right, kv_right,
    )
    given = (
        sums, pre_q, pre_k, p_q, p_k, b_q, b_k,
        query_full_weight, key_value_full_weight, mom_q, mom_k,
    )
    outs = pl.pallas_call(
        functools.partial(finish_kernel, nf),
        out_shape=(
            own_q, own_k, own_q, own_k, own_q, own_k,
            shape((QW, nf * QR), BF16), shape((nf * KR, KW), BF16),
        ),
        in_specs=[hbm] * 11,
        out_specs=(vmem,) * 8,
        scratch_shapes=[
            *(pltpu.VMEM(a.shape, a.dtype) for a in given),
            pltpu.VMEM((nf, QR, 256), BF16),
            dma((11,)),
        ],
    )(*given)
    return (*outs[:6], outs[6].T, outs[7])


def solution(mesh, dims=(4, 4, 16)):
    torus = Mesh(mesh.devices.reshape(*dims, 2), (*FS, *TP))
    placed = (P(FS, TP),) * 8 + (P(FS, None),) * 2 + (P(TP, None, None),) * 2
    return jax.shard_map(
        functools.partial(on_device, *dims),
        mesh=torus,
        in_specs=placed,
        out_specs=(P(FS, TP),) * 6 + (P(None, TP),) * 2,
        check_vma=False,
    )
```

time: 129 us -> 92.7 us (0.72)
  Pallas kernels: 122 us -> 91.9 us
  local copies, waits for them, and re-layouts: 6.63 us -> 0 us
    pallas_call x1, Pallas kernels: 119 us -> 87 us  [on_device(): pl.pallas_call(functools.partial(gather_kernel, ny, nx, nz), out_shape=(o...]
    unnamed x18 -> x0, local copies, waits for them, and re-layouts: 6.63 us -> none
    pallas_call x1, Pallas kernels: 3.05 us -> 4.86 us  [on_device(): pl.pallas_call(functools.partial(finish_kernel, nf), out_shape=(own_q, ow...]
where the time goes in v2:
time: 92.7 us; the launch traced here: 92.5 us
  Pallas kernels  91.9 us (99%)
    pallas_call x1, Pallas kernels, on_device(): pl.pallas_call(functools.partial(gather_kernel, ny, nx, nz), out_shape=(o...  87 us
    pallas_call x1, Pallas kernels, on_device(): pl.pallas_call(functools.partial(finish_kernel, nf), out_shape=(own_q, ow...  4.86 us

profile of v2, /device:TPU:1, one launch (start us, length us, event | category | flops | bytes accessed | tf_op | source)
XLA Modules:
  0.0 92.5 jit_solution(3613107710535323386)
XLA Ops:
  0.6 87.0 %shard_map.179 = (f32[96,192]{1,0:T(8,128)}, f32[64,256]{1,0:T(8,128)}, f32[96,192]{1,0:T(8,128)}, f32[64,256]{1,0:T(8,128)}, bf16[16,144,128]{2,1,0:T(8,128)(2,...) custom-call(bf16[48,1024]{1,0:T(8,128)(2,1)} %bitcast.5, ...), custom_call_target="tpu_custom_call" | custom-call | tf_op jit(solution)/shard_map/pallas_call | solution.py:494
  87.7 4.9 %shard_map.180 = (f32[96,192]{1,0:T(8,128)}, f32[64,256]{1,0:T(8,128)}, f32[96,192]{1,0:T(8,128)}, f32[64,256]{1,0:T(8,128)}, f32[96,192]{1,0:T(8,128)}, /*index...) custom-call(f32[1,128]{1,0:T(1,128)} %get-tuple-element.25.refs_0_, ...), custom_call_target="tpu_custom_call" | custom-call | tf_op jit(solution)/shard_map/pallas_call | solution.py:542

commit v3 on v2

--- a/solution.py
+++ b/solution.py
@@ -19,9 +19,9 @@
 QF, KF = 48, 32
 CF = QF + KF
 QP, KP = 144, 128
-PIECES = ((0, 32), (32, 48), (48, 80))
-N_Q_PIECES = 2
-DELAY = 2
+PIECES = tuple((r, r + 16) for r in range(0, CF, 16))
+N_Q_PIECES = 3
+REDUCE, OWN = 2, 4
 F32, BF16 = jnp.float32, jnp.bfloat16
 
 
@@ -47,6 +47,10 @@
 
 def pack_k(k):
     return jnp.concatenate([k[:, :128], k[:, 128:]], axis=0).astype(BF16)
+
+
+def farthest_first(n):
+    return sorted(range(1, n), key=lambda d: -min(d, n - d))
 
 
 def both(*conditions):
@@ -58,9 +62,9 @@
     latq, latk, cotq, h_cotk, h_wq, h_wk, h_momq, h_momk, h_leftq, h_leftk, h_rightq, h_rightk,
     o_momq, o_momk, o_preq, o_prek, o_pq, o_pk, o_bq, o_bk, o_sums,
     lat, cote, cotk, wq, wk, momq, momk, leftq, leftk, rightq, rightk,
-    outq, outk, rowq, rowk, midq, midk, ownq, ownk,
+    outq, outk, rowq, rowk, colq, colk, newq,
     halfq, halfk, wallq, wallk, pallq, pallk, hq, hk, s_a, s_b,
-    ring_recv, pair_recv, row_recv, col_recv, cast_recv, sems, load_sems,
+    ring_recv, pair_recv, sum_recv, row_recv, col_recv, cast_recv, sems, load_sems,
 ):
     nf = ny * nx
     top = nz // 2
@@ -68,9 +72,8 @@
     z, c = lax.axis_index("tp_0"), lax.axis_index("tp_1")
     fs = y * nx + x
     tp = z * 2 + c
-    ring_s, pair_s, g0q, g0k, g1q, g1k, r1q, r1k, a_s, a_r, b_s, b_r = [
-        sems.at[i] for i in range(12)
-    ]
+    (ring_s, pair_s, g0q, g0k, g1q, g1k, a_s, a_r, b_s, b_r,
+     h_sq, h_sk, h_rq, h_rk, m_sq, m_sk, m_rq, m_rk) = [sems.at[i] for i in range(18)]
 
     def row_peer(d):
         return {"fs_1": lax.rem(x + d, nx)}
@@ -95,8 +98,8 @@
                 (cotq, cote.at[:QW]),
                 (cotq.at[128:], cote.at[QW:]),
                 (h_cotk, cotk),
-                (h_momq, momq),
-                (h_momk, momk),
+                (h_momq, momq.at[y]),
+                (h_momk, momk.at[x]),
                 (h_leftq, leftq),
                 (h_leftk, leftk),
                 (h_rightq, rightq),
@@ -188,13 +191,15 @@
             wait(self.q.at[: nf - 1], self.sq)
             wait(self.k.at[: nf - 1], self.sk)
 
-    weights, halves, pres = Cast(0, wallq, wallk), Cast(1, halfq, halfk), Cast(2, pallq, pallk)
+    weights, pres = Cast(0, wallq, wallk), Cast(1, pallq, pallk)
     weights.start()
 
     for load in loads[4:]:
         load.wait()
-    delta = lax.rem(fs - z + nz, nz)
-    own_step = jnp.minimum(delta, nz - delta)
+    for d in range(1, ny):
+        send(momq.at[y], momq.at[y], m_sq, m_rq, col_peer(d))
+    for d in range(1, nx):
+        send(momk.at[x], momk.at[x], m_sk, m_rk, row_peer(d))
 
     def partial_gradient(slot, s):
         wait(lat.at[slot, 1 - c], pair_recv.at[slot])
@@ -232,111 +237,115 @@
         @pl.when(xs == x)
         def _():
             wait(rowq.at[ys, : nx - 1], pair_recv.at[nz + ys])
-            total = added(rowq, ys, nx).astype(BF16)
-
-            @pl.when(ys != y)
-            def _():
-                midq[ys] = total
-                send(midq.at[ys], ownq.at[0, y], g1q, r1q, {"fs_0": ys})
+            colq[ys, y] = added(rowq, ys, nx).astype(BF16)
+            for d in range(1, ny):
+                send(colq.at[ys, y], colq.at[ys, y], g1q, sum_recv.at[ys], col_peer(d))
+
+        @pl.when(ys == y)
+        def _():
+            wait(rowk.at[xs, : ny - 1], pair_recv.at[nz + ny + xs])
+            colk[xs, x] = added(rowk, xs, ny).astype(BF16)
+            for d in range(1, nx):
+                send(colk.at[xs, x], colk.at[xs, x], g1k, sum_recv.at[ny + xs], row_peer(d))
+
+    def momentum(slot, s):
+        ys, xs = s // nx, lax.rem(s, nx)
+
+        @pl.when(xs == x)
+        def _():
+            wait(colq.at[ys, : ny - 1], sum_recv.at[ys])
+            q = added(colq, ys, ny)
+            tail = q[QR:]
+            tail = jnp.concatenate([tail, pltpu.roll(tail, 64, 1)], axis=0)
+            newq[:, :128] = beta_mom * momq[ys, :, :128] + q[:QR]
+            newq[:, 128:] = beta_mom * momq[ys, :, 128:] + tail[:, :64]
+            halfq[s] = pack_q(dot(newq[...].astype(BF16), select))
+            for d in range(1, nx):
+                send(halfq.at[s], halfq.at[s], h_sq, h_rq, row_peer(d))
 
             @pl.when(ys == y)
             def _():
-                ownq[0, y] = total
+                o_momq[...] = newq[...]
 
         @pl.when(ys == y)
         def _():
-            wait(rowk.at[xs, : ny - 1], pair_recv.at[nz + ny + xs])
-            total = added(rowk, xs, ny).astype(BF16)
-
-            @pl.when(xs != x)
-            def _():
-                midk[xs] = total
-                send(midk.at[xs], ownk.at[0, x], g1k, r1k, {"fs_1": xs})
+            wait(colk.at[xs, : nx - 1], sum_recv.at[ny + xs])
+            k = added(colk, xs, nx)
+            new_a = beta_mom * momk[xs, :, :128] + k[:KR]
+            new_b = beta_mom * momk[xs, :, 128:] + k[KR:]
+            halfk[s] = jnp.concatenate([new_a, new_b], axis=0).astype(BF16)
+            for d in range(1, ny):
+                send(halfk.at[s], halfk.at[s], h_sk, h_rk, col_peer(d))
 
             @pl.when(xs == x)
             def _():
-                ownk[0, x] = total
-
-    def momentum():
-        wait(ownq.at[0, : ny - 1], r1q)
-        wait(ownk.at[0, : nx - 1], r1k)
-        q, k = added(ownq, 0, ny), added(ownk, 0, nx)
-        tail = q[QR:]
-        tail = jnp.concatenate([tail, pltpu.roll(tail, 64, 1)], axis=0)
-        o_momq[:, :128] = beta_mom * momq[:, :128] + q[:QR]
-        o_momq[:, 128:] = beta_mom * momq[:, 128:] + tail[:, :64]
-        o_momk[:, :128] = beta_mom * momk[:, :128] + k[:KR]
-        o_momk[:, 128:] = beta_mom * momk[:, 128:] + k[KR:]
-        halfq[fs] = pack_q(dot(o_momq[...].astype(BF16), select))
-        halfk[fs] = pack_k(o_momk[...])
-        halves.start()
-
-    def relay(slot, s):
-        ys, xs = s // nx, lax.rem(s, nx)
-
-        @pl.when(both(ys == y, xs != x))
-        def _():
-            halves.pass_q(xs)
-
-        @pl.when(both(xs == x, ys != y))
-        def _():
-            halves.pass_k(ys)
-
-    def per_slot(do, st):
-        @pl.when(both(st >= 1, st <= top))
-        def _():
-            do(2 * st - 1, lax.rem(z + nz - st, nz))
-
-        @pl.when(both(st >= 0, st < top))
-        def _():
-            do(2 * st, lax.rem(z + st, nz))
+                o_momk[:, :128] = new_a
+                o_momk[:, 128:] = new_b
+
+    def per_slot(st):
+        def first(do):
+            @pl.when(both(st >= 1, st <= top))
+            def _():
+                do(2 * st - 1, lax.rem(z + nz - st, nz))
+
+        def second(do):
+            @pl.when(both(st >= 0, st < top))
+            def _():
+                do(2 * st, lax.rem(z + st, nz))
+
+        return first, second
+
+    def ring(k, p):
+        is_q = p < N_Q_PIECES
+        a, b = 2 * k - 1, jnp.minimum(2 * k, nz - 1)
+        last_a, last_b = (top, top - 1) if is_q else (top - 1, top)
+
+        @pl.when(k <= last_a)
+        def _():
+            wait(part(a, p), ring_recv.at[a, p])
+
+            @pl.when(k < last_a)
+            def _():
+                forward(a, a + 2, p, up)
+
+            share(a, p)
+
+        @pl.when(k <= last_b)
+        def _():
+            wait(part(b, p), ring_recv.at[b, p])
+
+            @pl.when(k < last_b)
+            def _():
+                forward(b, jnp.minimum(b + 2, nz - 1), p, down)
+
+            share(b, p)
 
     def step(k, carry):
-        for p in range(len(PIECES)):
-            is_q = p < N_Q_PIECES
-            a, b = 2 * k - 1, jnp.minimum(2 * k, nz - 1)
-            last_a, last_b = (top, top - 1) if is_q else (top - 1, top)
-
-            @pl.when(k <= last_a)
-            def _():
-                wait(part(a, p), ring_recv.at[a, p])
-
-                @pl.when(k < last_a)
-                def _():
-                    forward(a, a + 2, p, up)
-
-                share(a, p)
-
-            @pl.when(k <= last_b)
-            def _():
-                wait(part(b, p), ring_recv.at[b, p])
-
-                @pl.when(k < last_b)
-                def _():
-                    forward(b, jnp.minimum(b + 2, nz - 1), p, down)
-
-                share(b, p)
-
-        for i in range(1, max(nx, ny)):
-
-            @pl.when(k == i + 2)
-            def _():
-                if i < nx:
-                    weights.pass_q(lax.rem(x + i, nx))
-                if i < ny:
-                    weights.pass_k(lax.rem(y + i, ny))
-
-        per_slot(partial_gradient, k - 1)
-        per_slot(reduce_first, k - 1 - DELAY)
-
-        @pl.when(k == own_step + 1 + 2 * DELAY)
-        def _():
-            momentum()
-
-        per_slot(relay, k - 1 - 3 * DELAY)
+        first, second = per_slot(k - 1)
+        ring(k, 0)
+        first(partial_gradient)
+        ring(k, 1)
+        for which in per_slot(k - 1 - REDUCE):
+            which(reduce_first)
+        ring(k, 2)
+        second(partial_gradient)
+        ring(k, 3)
+        ring(k, 4)
+
+        @pl.when(k == 3)
+        def _():
+            wait(momq.at[: ny - 1], m_rq)
+            wait(momk.at[: nx - 1], m_rk)
+            for i in range(1, nx):
+                weights.pass_q(lax.rem(x + i, nx))
+            for i in range(1, ny):
+                weights.pass_k(lax.rem(y + i, ny))
+
+        for which in per_slot(k - 1 - OWN):
+            which(momentum)
         return carry
 
-    lax.fori_loop(1, max(top + 2 + 3 * DELAY, max(nx, ny) + 2), step, 0)
+    lax.fori_loop(1, top + 2 + OWN, step, 0)
 
     weights.finish()
     w_out = [
@@ -345,7 +354,8 @@
     ]
     for copy in w_out:
         copy.start()
-    halves.finish()
+    wait(halfq.at[: (nx - 1) * ny], h_rq)
+    wait(halfk.at[: (ny - 1) * nx], h_rk)
 
     def spread(s, carry):
         tail = halfq[s, QR:, :]
@@ -384,7 +394,7 @@
         t = lax.rem(tp + d, 2 * nz)
         return {"tp_0": t // 2, "tp_1": lax.rem(t, 2)}
 
-    for d in range(1, 2 * nz):
+    for d in farthest_first(2 * nz):
         send(s_b.at[tp], s_b.at[tp], b_s, b_r, column(d))
     for i in range(1, nx):
         pres.pass_q(lax.rem(x + i, nx))
@@ -401,10 +411,13 @@
     wait(lat.at[:, 0], pair_s)
     wait(outq.at[: nf - ny], g0q)
     wait(outk.at[: nf - nx], g0k)
-    wait(midq.at[: ny - 1], g1q)
-    wait(midk.at[: nx - 1], g1k)
+    wait(outq.at[: ny * (ny - 1)], g1q)
+    wait(outk.at[: nx * (nx - 1)], g1k)
+    wait(outq.at[: ny * (nx - 1)], h_sq)
+    wait(outk.at[: nx * (ny - 1)], h_sk)
+    wait(momq.at[: ny - 1], m_sq)
+    wait(momk.at[: nx - 1], m_sk)
     weights.drain()
-    halves.drain()
     pres.drain()
     for copy in (*w_out, *p_out):
         copy.wait()
@@ -502,8 +515,8 @@
             pltpu.VMEM((tokens, KW), BF16),
             pltpu.VMEM((QR, QW), F32),
             pltpu.VMEM((KR, KW), F32),
-            pltpu.VMEM((QR, QW), F32),
-            pltpu.VMEM((KR, KW), F32),
+            pltpu.VMEM((ny, QR, QW), F32),
+            pltpu.VMEM((nx, KR, KW), F32),
             pltpu.VMEM((QR, nf * QR), BF16),
             pltpu.VMEM((KR, nf * KR), BF16),
             pltpu.VMEM((1, QW, QW), BF16),
@@ -512,10 +525,9 @@
             block_k(nz),
             block_q(ny, nx),
             block_k(nx, ny),
-            block_q(ny),
-            block_k(nx),
-            block_q(1, ny),
-            block_k(1, nx),
+            block_q(ny, ny),
+            block_k(nx, nx),
+            pltpu.VMEM((QR, QW), F32),
             *(block_q(nf), block_k(nf)) * 3,
             pltpu.VMEM((nf, QR, 256), BF16),
             pltpu.VMEM((nf, KR, 256), BF16),
@@ -523,10 +535,11 @@
             pltpu.VMEM((2 * nz, 1, 128), F32),
             dma((nz, len(PIECES))),
             dma((nz + ny + nx,)),
-            dma((3, nx)),
-            dma((3, ny)),
-            dma((3, 4)),
-            dma((12,)),
+            dma((ny + nx,)),
+            dma((2, nx)),
+            dma((2, ny)),
+            dma((2, 4)),
+            dma((18,)),
             dma((13,)),
         ],
         compiler_params=pltpu.CompilerParams(collective_id=0, has_side_effects=True),

time: 92.7 us -> 86.5 us (0.933)
  Pallas kernels: 91.9 us -> 85.6 us
    pallas_call x1, Pallas kernels: 87 us -> 80.8 us  [on_device(): pl.pallas_call(functools.partial(gather_kernel, ny, nx, nz), out_shape=(o...]
where the time goes in v3:
time: 86.5 us; the launch traced here: 86.3 us
  Pallas kernels  85.6 us (99%)
    pallas_call x1, Pallas kernels, on_device(): pl.pallas_call(functools.partial(gather_kernel, ny, nx, nz), out_shape=(o...  80.8 us
    pallas_call x1, Pallas kernels, on_device(): pl.pallas_call(functools.partial(finish_kernel, nf), out_shape=(own_q, ow...  4.86 us

profile of v3, /device:TPU:1, one launch (start us, length us, event | category | flops | bytes accessed | tf_op | source)
XLA Modules:
  0.0 86.3 jit_solution(10336846732542326838)
XLA Ops:
  0.6 80.8 %shard_map.179 = (f32[96,192]{1,0:T(8,128)}, f32[64,256]{1,0:T(8,128)}, f32[96,192]{1,0:T(8,128)}, f32[64,256]{1,0:T(8,128)}, bf16[16,144,128]{2,1,0:T(8,128)(2,...) custom-call(bf16[48,1024]{1,0:T(8,128)(2,1)} %bitcast.5, ...), custom_call_target="tpu_custom_call" | custom-call | tf_op jit(solution)/shard_map/pallas_call | solution.py:507
  81.4 4.9 %shard_map.180 = (f32[96,192]{1,0:T(8,128)}, f32[64,256]{1,0:T(8,128)}, f32[96,192]{1,0:T(8,128)}, f32[64,256]{1,0:T(8,128)}, f32[96,192]{1,0:T(8,128)}, /*index...) custom-call(f32[1,128]{1,0:T(1,128)} %get-tuple-element.25.refs_0_, ...), custom_call_target="tpu_custom_call" | custom-call | tf_op jit(solution)/shard_map/pallas_call | solution.py:555

commit v4 on v3

--- a/solution.py
+++ b/solution.py
@@ -39,6 +39,16 @@
     return jnp.where(row == jnp.where(col < QW, col, col - 64), 1.0, 0.0).astype(BF16)
 
 
+def split_halves(n):
+    col = lax.broadcasted_iota(jnp.int32, (1, n), 1)
+    second = (col >= n // 2).astype(jnp.int32)
+    col = col - second * (n // 2)
+    block = sum((col >= i).astype(jnp.int32) for i in range(QR // 2, n // 2, QR // 2))
+    source = col + (block + second) * (QR // 2)
+    row = lax.broadcasted_iota(jnp.int32, (n, n), 0)
+    return jnp.where(row == source, 1.0, 0.0).astype(BF16)
+
+
 def pack_q(q):
     lane = lax.broadcasted_iota(jnp.int32, (QR // 2, 128), 1)
     tail = jnp.where(lane < 64, q[: QR // 2, 128:], q[QR // 2 :, 128:])
@@ -60,10 +70,11 @@
 def gather_kernel(
     ny, nx, nz,
     latq, latk, cotq, h_cotk, h_wq, h_wk, h_momq, h_momk, h_leftq, h_leftk, h_rightq, h_rightk,
-    o_momq, o_momk, o_preq, o_prek, o_pq, o_pk, o_bq, o_bk, o_sums,
+    to_momq, to_momk, to_preq, to_prek, to_pq, to_pk, to_bq, to_bk, o_sums,
     lat, cote, cotk, wq, wk, momq, momk, leftq, leftk, rightq, rightk,
     outq, outk, rowq, rowk, colq, colk, newq,
-    halfq, halfk, wallq, wallk, pallq, pallk, hq, hk, s_a, s_b,
+    halfq, halfk, wallq, wallk, pallq, pallk, o_momq, o_momk, o_preq, o_prek,
+    left_lo, left_hi, right_q, spread, bq, bk, pq, pk, s_a, s_b,
     ring_recv, pair_recv, sum_recv, row_recv, col_recv, cast_recv, sems, load_sems,
 ):
     nf = ny * nx
@@ -118,11 +129,8 @@
 
     select = repeat_tail()
 
-    for load in loads[:4]:
+    for load in loads[:2]:
         load.wait()
-    wallq[fs] = pack_q(dot(wq[...].astype(BF16), select))
-    wallk[fs] = pack_k(wk[...])
-
     pl.semaphore_wait(barrier, 3 + nf - 1)
 
     def send(src, dst, s_sem, r_sem, to):
@@ -159,11 +167,11 @@
             self.sq, self.sk, self.rq, self.rk = [cast_recv.at[which, i] for i in range(4)]
 
         def along_x(self, block, s_sem, r_sem):
-            for d in range(1, nx):
+            for d in farthest_first(nx):
                 send(block, block, s_sem, r_sem, row_peer(d))
 
         def along_y(self, block, s_sem, r_sem):
-            for d in range(1, ny):
+            for d in farthest_first(ny):
                 send(block, block, s_sem, r_sem, col_peer(d))
 
         def start(self):
@@ -192,14 +200,23 @@
             wait(self.k.at[: nf - 1], self.sk)
 
     weights, pres = Cast(0, wallq, wallk), Cast(1, pallq, pallk)
+    for load in loads[2:]:
+        load.wait()
+    wallq[fs] = pack_q(dot(wq[...].astype(BF16), select))
+    wallk[fs] = pack_k(wk[...])
     weights.start()
-
-    for load in loads[4:]:
-        load.wait()
-    for d in range(1, ny):
+    for d in farthest_first(ny):
         send(momq.at[y], momq.at[y], m_sq, m_rq, col_peer(d))
-    for d in range(1, nx):
+    for d in farthest_first(nx):
         send(momk.at[x], momk.at[x], m_sk, m_rk, row_peer(d))
+
+    right_q[...] = dot(rightq[0], select).astype(BF16)
+    group = min(8, nf) * QR
+    split = split_halves(group)
+    for at in range(0, nf * QR // group):
+        cut = dot(leftq[:, at * group : (at + 1) * group], split).astype(BF16)
+        left_lo[:, at * group // 2 : (at + 1) * group // 2] = cut[:, : group // 2]
+        left_hi[:, at * group // 2 : (at + 1) * group // 2] = cut[:, group // 2 :]
 
     def partial_gradient(slot, s):
         wait(lat.at[slot, 1 - c], pair_recv.at[slot])
@@ -238,14 +255,14 @@
         def _():
             wait(rowq.at[ys, : nx - 1], pair_recv.at[nz + ys])
             colq[ys, y] = added(rowq, ys, nx).astype(BF16)
-            for d in range(1, ny):
+            for d in farthest_first(ny):
                 send(colq.at[ys, y], colq.at[ys, y], g1q, sum_recv.at[ys], col_peer(d))
 
         @pl.when(ys == y)
         def _():
             wait(rowk.at[xs, : ny - 1], pair_recv.at[nz + ny + xs])
             colk[xs, x] = added(rowk, xs, ny).astype(BF16)
-            for d in range(1, nx):
+            for d in farthest_first(nx):
                 send(colk.at[xs, x], colk.at[xs, x], g1k, sum_recv.at[ny + xs], row_peer(d))
 
     def momentum(slot, s):
@@ -260,7 +277,7 @@
             newq[:, :128] = beta_mom * momq[ys, :, :128] + q[:QR]
             newq[:, 128:] = beta_mom * momq[ys, :, 128:] + tail[:, :64]
             halfq[s] = pack_q(dot(newq[...].astype(BF16), select))
-            for d in range(1, nx):
+            for d in farthest_first(nx):
                 send(halfq.at[s], halfq.at[s], h_sq, h_rq, row_peer(d))
 
             @pl.when(ys == y)
@@ -274,7 +291,7 @@
             new_a = beta_mom * momk[xs, :, :128] + k[:KR]
             new_b = beta_mom * momk[xs, :, 128:] + k[KR:]
             halfk[s] = jnp.concatenate([new_a, new_b], axis=0).astype(BF16)
-            for d in range(1, ny):
+            for d in farthest_first(ny):
                 send(halfk.at[s], halfk.at[s], h_sk, h_rk, col_peer(d))
 
             @pl.when(xs == x)
@@ -347,43 +364,76 @@
 
     lax.fori_loop(1, top + 2 + OWN, step, 0)
 
+    outs = []
+
+    def write(src, dst):
+        outs.append(pltpu.make_async_copy(src, dst, load_sems.at[len(outs)]))
+        outs[-1].start()
+
+    row = lax.broadcasted_iota(jnp.int32, (QW, 256), 0)
+    col = lax.broadcasted_iota(jnp.int32, (QW, 256), 1)
+    eye = jnp.where(row == col, 1.0, 0.0).astype(BF16)
+
+    def laid_out(q, k, to_q, to_k):
+        def block(s, carry):
+            tail = q[s, QR:, :]
+            spread[s, :, :128] = q[s, :QR, :]
+            spread[s, : QR // 2, 128:] = tail
+            spread[s, QR // 2 :, 128:] = pltpu.roll(tail.astype(F32), 64, 1).astype(BF16)
+            rows = pl.ds(pl.multiple_of(s * KR, KR), KR)
+            to_k[rows, :128] = k[s, :KR, :]
+            to_k[rows, 128:] = k[s, KR:, :]
+            return carry
+
+        lax.fori_loop(0, nf, block, 0, unroll=2)
+        to_q[...] = dot_t(eye, spread[...].reshape(nf * QR, 256)).astype(BF16)
+
     weights.finish()
-    w_out = [
-        pltpu.make_async_copy(wallq, o_bq, load_sems.at[0]),
-        pltpu.make_async_copy(wallk, o_bk, load_sems.at[1]),
-    ]
-    for copy in w_out:
-        copy.start()
+    laid_out(wallq, wallk, bq, bk)
+    write(bq, to_bq)
+    write(bk, to_bk)
+    write(o_momq, to_momq)
+    write(o_momk, to_momk)
+    lane = lax.broadcasted_iota(jnp.int32, (1, 128), 1)
+
+    def with_squares(sums, values, first):
+        for i, v in enumerate(values):
+            sums = jnp.where(lane == first + i, jnp.sum(v * v), sums)
+        return sums
+
+    sums = with_squares(jnp.zeros((1, 128), F32), (o_momq[...], o_momk[...]), 0)
     wait(halfq.at[: (nx - 1) * ny], h_rq)
     wait(halfk.at[: (ny - 1) * nx], h_rk)
-
-    def spread(s, carry):
-        tail = halfq[s, QR:, :]
-        hq[s, :, :128] = halfq[s, :QR, :]
-        hq[s, : QR // 2, 128:] = tail
-        hq[s, QR // 2 :, 128:] = pltpu.roll(tail.astype(F32), 64, 1).astype(BF16)
-        hk[s, :, :128] = halfk[s, :KR, :]
-        hk[s, :, 128:] = halfk[s, KR:, :]
-        return carry
-
-    lax.fori_loop(0, nf, spread, 0)
-    left_q = dot(leftq[...], hq[...].reshape(nf * QR, 256))[:, :QW].astype(BF16)
-    left_k = dot(leftk[...], hk[...].reshape(nf * KR, 256)).astype(BF16)
-    right_q = dot(rightq[0], select).astype(BF16)
-    pre_q = dot(left_q, right_q)
-    pre_k = dot(left_k, rightk[0])
+    tail = halfq[:, QR:, :].reshape(nf * QR // 2, 128)
+    left_q = jnp.concatenate(
+        [
+            dot(leftq[...], halfq[:, :QR, :].reshape(nf * QR, 128)),
+            dot(left_lo[...], tail) + pltpu.roll(dot(left_hi[...], tail), 64, 1),
+        ],
+        axis=1,
+    )
+    left_k = jnp.concatenate(
+        [
+            dot(leftk[...], halfk[:, :KR, :].reshape(nf * KR, 128)),
+            dot(leftk[...], halfk[:, KR:, :].reshape(nf * KR, 128)),
+        ],
+        axis=1,
+    )
+    pre_q = dot(left_q[:, :QW].astype(BF16), right_q[...])
+    pre_k = dot(left_k.astype(BF16), rightk[0])
+    s_a[fs] = with_squares(sums, (pre_q[:, :QW], pre_k), 2)
+    for dy, dx in sorted(
+        ((dy, dx) for dy in range(ny) for dx in range(nx) if dy or dx),
+        key=lambda d: -min(d[0], ny - d[0]) - min(d[1], nx - d[1]),
+    ):
+        send(s_a.at[fs], s_a.at[fs], a_s, a_r, {**col_peer(dy), **row_peer(dx)})
     pallq[fs] = pack_q(pre_q)
     pallk[fs] = pack_k(pre_k)
+    pres.start()
     o_preq[...] = pre_q[:, :QW]
     o_prek[...] = pre_k
-    lane = lax.broadcasted_iota(jnp.int32, (1, 128), 1)
-    sums = jnp.zeros((1, 128), F32)
-    for i, v in enumerate((o_momq[...], o_momk[...], pre_q[:, :QW], pre_k)):
-        sums = jnp.where(lane == i, jnp.sum(v * v), sums)
-    s_a[fs] = sums
-    for d in range(1, nf):
-        send(s_a.at[fs], s_a.at[fs], a_s, a_r, plane(d))
-    pres.start()
+    write(o_preq, to_preq)
+    write(o_prek, to_prek)
     wait(s_a.at[: nf - 1], a_r)
     total = s_a[0]
     for i in range(1, nf):
@@ -401,12 +451,9 @@
     for i in range(1, ny):
         pres.pass_k(lax.rem(y + i, ny))
     pres.finish()
-    p_out = [
-        pltpu.make_async_copy(pallq, o_pq, load_sems.at[2]),
-        pltpu.make_async_copy(pallk, o_pk, load_sems.at[3]),
-    ]
-    for copy in p_out:
-        copy.start()
+    laid_out(pallq, pallk, pq, pk)
+    write(pq, to_pq)
+    write(pk, to_pk)
     wait(lat.at[: nz - 1, 0], ring_s)
     wait(lat.at[:, 0], pair_s)
     wait(outq.at[: nf - ny], g0q)
@@ -419,7 +466,7 @@
     wait(momk.at[: nx - 1], m_sk)
     weights.drain()
     pres.drain()
-    for copy in (*w_out, *p_out):
+    for copy in outs:
         copy.wait()
     wait(s_a.at[: nf - 1], a_s)
     wait(s_b.at[: 2 * nz - 1], b_s)
@@ -430,53 +477,64 @@
     o_sums[...] = total
 
 
-def finish_kernel(
-    nf, *refs,
-):
+def finish_kernel(nf, *refs):
     given, outs, held = refs[:11], refs[11:19], refs[19:30]
-    cq, load_sems = refs[30:]
-    o_momq, o_momk, o_updq, o_updk, o_wq, o_wk, o_cq, o_ck = outs
+    upd_q, upd_k, new_wq, new_wk, copy_q, copy_k, load_sems, out_sems = refs[30:]
+    to_momq, to_momk, to_updq, to_updk, to_wq, to_wk, to_cq, to_ck = outs
     loads = [
         pltpu.make_async_copy(src, dst, load_sems.at[i])
         for i, (src, dst) in enumerate(zip(given, held))
     ]
     for load in loads:
         load.start()
-    row = lax.broadcasted_iota(jnp.int32, (QW, 256), 0)
-    col = lax.broadcasted_iota(jnp.int32, (QW, 256), 1)
-    eye = jnp.where(row == col, 1.0, 0.0).astype(BF16)
-    for load in loads:
-        load.wait()
-    sums, preq, prek, pq, pk, bq, bk, wq, wk, momq, momk = held
+    sums, momq, momk, preq, prek, wq, wk, bq, pq, bk, pk = held
+    started = []
+
+    def write(src, dst):
+        started.append(pltpu.make_async_copy(src, dst, out_sems.at[len(started)]))
+        started[-1].start()
+
+    loads[0].wait()
     v = sums[...]
     lane = lax.broadcasted_iota(jnp.int32, (1, 128), 1)
     scales = jnp.sqrt(v / pltpu.roll(v, 126, 1))
     scale_q, scale_k = [
         jnp.sum(jnp.where(lane == i, scales, 0.0), axis=1, keepdims=True) for i in (0, 1)
     ]
-    o_momq[...] = momq[...]
-    o_momk[...] = momk[...]
-    upd_q = scale_q * preq[...]
-    upd_k = scale_k * prek[...]
-    o_updq[...] = upd_q
-    o_updk[...] = upd_k
-    o_wq[...] = wq[...] - learn_rate * upd_q
-    o_wk[...] = wk[...] - learn_rate * upd_k
-
-    def body(s, carry):
-        q = bq[s].astype(F32) - learn_rate * (scale_q * pq[s].astype(F32))
-        k = bk[s].astype(F32) - learn_rate * (scale_k * pk[s].astype(F32))
-        tail = q[QR:]
-        cq[s, :, :128] = q[:QR].astype(BF16)
-        cq[s, : QR // 2, 128:] = tail.astype(BF16)
-        cq[s, QR // 2 :, 128:] = pltpu.roll(tail, 64, 1).astype(BF16)
-        rows = pl.ds(pl.multiple_of(s * KR, KR), KR)
-        o_ck[rows, :128] = k[:KR].astype(BF16)
-        o_ck[rows, 128:] = k[KR:].astype(BF16)
+    for load in loads[1:9]:
+        load.wait()
+    write(momq, to_momq)
+    write(momk, to_momk)
+
+    def query(i, carry):
+        rows = pl.ds(pl.multiple_of(i * 32, 32), 32)
+        step = learn_rate * (scale_q * pq[rows, :].astype(F32))
+        copy_q[rows, :] = (bq[rows, :].astype(F32) - step).astype(BF16)
         return carry
 
-    lax.fori_loop(0, nf, body, 0)
-    o_cq[...] = dot_t(eye, cq[...].reshape(nf * QR, 256)).astype(BF16)
+    lax.fori_loop(0, QW // 32, query, 0)
+    write(copy_q, to_cq)
+    for load in loads[9:]:
+        load.wait()
+
+    def key_value(s, carry):
+        rows = pl.ds(pl.multiple_of(s * 128, 128), 128)
+        step = learn_rate * (scale_k * pk[rows, :].astype(F32))
+        copy_k[rows, :] = (bk[rows, :].astype(F32) - step).astype(BF16)
+        return carry
+
+    lax.fori_loop(0, nf * KR // 128, key_value, 0)
+    write(copy_k, to_ck)
+    upd_q[...] = scale_q * preq[...]
+    upd_k[...] = scale_k * prek[...]
+    new_wq[...] = wq[...] - learn_rate * upd_q[...]
+    new_wk[...] = wk[...] - learn_rate * upd_k[...]
+    write(upd_q, to_updq)
+    write(upd_k, to_updk)
+    write(new_wq, to_wq)
+    write(new_wk, to_wk)
+    for copy in started:
+        copy.wait()
 
 
 def on_device(
@@ -499,7 +557,7 @@
     vmem = pl.BlockSpec(memory_space=pltpu.VMEM)
     shape = jax.ShapeDtypeStruct
     own_q, own_k = shape((QR, QW), F32), shape((KR, KW), F32)
-    all_q, all_k = shape((nf, QP, 128), BF16), shape((nf, KP, 128), BF16)
+    all_q, all_k = shape((QW, nf * QR), BF16), shape((nf * KR, KW), BF16)
     row = shape((1, 128), F32)
     hbm = pl.BlockSpec(memory_space=pltpu.HBM)
     block_q, block_k = [lambda *n, r=r: pltpu.VMEM((*n, r, 128), BF16) for r in (QP, KP)]
@@ -508,7 +566,7 @@
         functools.partial(gather_kernel, ny, nx, nz),
         out_shape=(own_q, own_k, own_q, own_k, all_q, all_k, all_q, all_k, row),
         in_specs=[hbm] * 12,
-        out_specs=(vmem,) * 4 + (hbm,) * 4 + (vmem,),
+        out_specs=(hbm,) * 8 + (vmem,),
         scratch_shapes=[
             pltpu.VMEM((nz, 2, CF, tokens), BF16),
             pltpu.VMEM((256, tokens), BF16),
@@ -529,8 +587,15 @@
             block_k(nx, nx),
             pltpu.VMEM((QR, QW), F32),
             *(block_q(nf), block_k(nf)) * 3,
+            pltpu.VMEM((QR, QW), F32),
+            pltpu.VMEM((KR, KW), F32),
+            pltpu.VMEM((QR, QW), F32),
+            pltpu.VMEM((KR, KW), F32),
+            pltpu.VMEM((QR, nf * QR // 2), BF16),
+            pltpu.VMEM((QR, nf * QR // 2), BF16),
+            pltpu.VMEM((QW, 256), BF16),
             pltpu.VMEM((nf, QR, 256), BF16),
-            pltpu.VMEM((nf, KR, 256), BF16),
+            *(pltpu.VMEM((QW, nf * QR), BF16), pltpu.VMEM((nf * KR, KW), BF16)) * 2,
             pltpu.VMEM((nf, 1, 128), F32),
             pltpu.VMEM((2 * nz, 1, 128), F32),
             dma((nz, len(PIECES))),
@@ -549,8 +614,8 @@
         query_left, kv_left, query_right, kv_right,
     )
     given = (
-        sums, pre_q, pre_k, p_q, p_k, b_q, b_k,
-        query_full_weight, key_value_full_weight, mom_q, mom_k,
+        sums, mom_q, mom_k, pre_q, pre_k, query_full_weight, key_value_full_weight,
+        b_q, p_q, b_k, p_k,
     )
     outs = pl.pallas_call(
         functools.partial(finish_kernel, nf),
@@ -559,11 +624,17 @@
             shape((QW, nf * QR), BF16), shape((nf * KR, KW), BF16),
         ),
         in_specs=[hbm] * 11,
-        out_specs=(vmem,) * 8,
+        out_specs=(hbm,) * 8,
         scratch_shapes=[
             *(pltpu.VMEM(a.shape, a.dtype) for a in given),
-            pltpu.VMEM((nf, QR, 256), BF16),
+            pltpu.VMEM((QR, QW), F32),
+            pltpu.VMEM((KR, KW), F32),
+            pltpu.VMEM((QR, QW), F32),
+            pltpu.VMEM((KR, KW), F32),
+            pltpu.VMEM((QW, nf * QR), BF16),
+            pltpu.VMEM((nf * KR, KW), BF16),
             dma((11,)),
+            dma((8,)),
         ],
     )(*given)
     return (*outs[:6], outs[6].T, outs[7])

time: 86.5 us -> 82.3 us (0.951)
  Pallas kernels: 85.6 us -> 81.5 us
    pallas_call x1, Pallas kernels: 80.8 us -> 78.4 us  [on_device(): pl.pallas_call(functools.partial(gather_kernel, ny, nx, nz), out_shape=(o...]
    pallas_call x1, Pallas kernels: 4.86 us -> 3.1 us  [on_device(): pl.pallas_call(functools.partial(finish_kernel, nf), out_shape=(own_q, ow...]
where the time goes in v4:
time: 82.3 us; the launch traced here: 82.1 us
  Pallas kernels  81.5 us (99%)
    pallas_call x1, Pallas kernels, on_device(): pl.pallas_call(functools.partial(gather_kernel, ny, nx, nz), out_shape=(o...  78.4 us
    pallas_call x1, Pallas kernels, on_device(): pl.pallas_call(functools.partial(finish_kernel, nf), out_shape=(own_q, ow...  3.1 us

profile of v4, /device:TPU:1, one launch (start us, length us, event | category | flops | bytes accessed | tf_op | source)
XLA Modules:
  0.0 82.1 jit_solution(15672177286309670587)
XLA Ops:
  0.6 78.4 %shard_map.179 = (f32[96,192]{1,0:T(8,128)}, f32[64,256]{1,0:T(8,128)}, f32[96,192]{1,0:T(8,128)}, f32[64,256]{1,0:T(8,128)}, bf16[192,1536]{1,0:T(8,128)(2,1)},...) custom-call(bf16[48,1024]{1,0:T(8,128)(2,1)} %bitcast.5, ...), custom_call_target="tpu_custom_call" | custom-call | tf_op jit(solution)/shard_map/pallas_call | solution.py:565
  79.0 3.1 %shard_map.180 = (f32[96,192]{1,0:T(8,128)}, f32[64,256]{1,0:T(8,128)}, f32[96,192]{1,0:T(8,128)}, f32[64,256]{1,0:T(8,128)}, f32[96,192]{1,0:T(8,128)}, /*index...) custom-call(f32[1,128]{1,0:T(1,128)} %get-tuple-element.25.refs_0_, ...), custom_call_target="tpu_custom_call" | custom-call | tf_op jit(solution)/shard_map/pallas_call | solution.py:620
